TPU v7x, 512 devices: a whole 4x8x8 slice. The times are simulated.
512 devices in a mesh: sp: 32 (over z, x), dp: 16 (over y, core).
Axes of the slice: x: 4, y: 8, z: 8, core: 2. Of those that a mesh axis runs over, the one named last changes fastest.
Arguments:
- query_rows: bfloat16 [16, 4096, 2048], P('dp', 'sp'), may hold values from -6 to 6
- key_rows: bfloat16 [16, 4096, 2048], P('dp', 'sp'), may hold values from -6 to 6
- value_rows: bfloat16 [16, 4096, 2048], P('dp', 'sp'), may hold values from -6 to 6
- decay_low: bfloat16 [16, 4096, 128], P('dp', 'sp'), may hold values from -5 to 5
- rate_low: bfloat16 [16, 4096, 128], P('dp', 'sp'), may hold values from -4 to 4
- decay_up: bfloat16 [128, 2048], replicated, may hold values from -0.5 to 0.5
- rate_up: bfloat16 [128, 2048], replicated, may hold values from -0.5 to 0.5
- decay_base: float32 [2048], replicated, may hold values from -12 to -2
- norm_gain: float32 [2048], replicated, may hold values from 0.1 to 1.9
- out_weight: bfloat16 [2048, 2048], P(None, 'dp'), may hold values from -0.125 to 0.125
Outputs:
- layer_out: bfloat16 [16, 4096, 2048], P('dp', 'sp')
All inputs are finite; a program needn't handle non-finite values.
Results may differ from a plain program's by a relative error of at most 0.005.
Values may be sent and summed in bfloat16 or wider, within the bound.
No kernel may reach another device: no remote copies, remote signals or barrier semaphores. Data moves between devices by JAX's collectives and lax.ppermute only.
A program may use at most 128 MiB of HBM per device.

v0:
```python
import jax
import jax.numpy as jnp
from jax import lax
from jax.experimental import pallas as pl
from jax.experimental.pallas import tpu as pltpu
from jax.sharding import Mesh
from jax.sharding import PartitionSpec as P

HEAD = 64
PAIR = 2 * HEAD
DP = ("dp_0", "dp_1")
GROUP = 4
F32 = jnp.float32
BF16 = jnp.bfloat16


def dot(left, right):
    return lax.dot_general(left, right, (((1,), (0,)), ((), ())), preferred_element_type=F32)


def dot_nt(left, right):
    return lax.dot_general(left, right, (((1,), (1,)), ((), ())), preferred_element_type=F32)


def split(value):
    high = value.astype(BF16)
    low = (value - high.astype(F32)).astype(BF16)
    return high, low


def lanes(*parts):
    return jnp.concatenate(parts, axis=1)


def rows(*parts):
    return jnp.concatenate(parts, axis=0)


def half_turn(value):
    return pltpu.roll(value, HEAD, 1)


def product(left, right):
    left_high, left_low = left
    right_high, right_low = right
    return dot(lanes(left_high, left_low), rows(right_high, right_high)) + dot(left_high, right_low)


def iota(shape, dim):
    return lax.broadcasted_iota(jnp.int32, shape, dim)


def same_head():
    return (iota((PAIR, PAIR), 0) // HEAD == iota((PAIR, PAIR), 1) // HEAD).astype(F32).astype(BF16)


def inverses(matrices, length):
    row = iota((length, length), 0)
    col = iota((length, length), 1)
    apart = row ^ col
    eye = (row == col).astype(F32)
    pieces = [split(m) for m in matrices]
    solved = [eye - jnp.where(apart == 1, m, 0.0) for m in matrices]
    block = 2
    while block < length:
        here = (apart >= block) & (apart < 2 * block)
        parts = [split(s) for s in solved]
        masked = [
            (jnp.where(here, h, jnp.zeros_like(h)), jnp.where(here, l, jnp.zeros_like(l)))
            for h, l in pieces
        ]
        inner = [split(product(c, x)) for c, x in zip(masked, parts)]
        solved = [s - product(x, d) for s, x, d in zip(solved, parts, inner)]
        block *= 2
    return [split(s) for s in solved]


def local_kernel(q_ref, k_ref, v_ref, dl_ref, rl_ref, du_ref, ru_ref, base_ref, msg_ref, r_ref, o_ref):
    length = q_ref.shape[0]
    row = iota((length, length), 0)
    col = iota((length, length), 1)
    strict = row > col
    within = row >= col
    lower = within.astype(F32).astype(BF16)
    lower_twice = lanes(lower, lower)
    ones = same_head()
    ones_twice = rows(ones, ones)
    squashed = jnp.tanh(dl_ref[...].astype(F32)).astype(BF16)
    decay_pre = (base_ref[...] + dot(squashed, du_ref[...])).astype(BF16).astype(F32)
    rate_pre = dot(rl_ref[...], ru_ref[...]).astype(BF16).astype(F32)
    decays = (-0.6065306597126334) / (1.0 + jnp.exp(-decay_pre))
    rates = 0.5 + 0.5 * jnp.tanh(0.5 * rate_pre)
    first = iota((length, PAIR), 1) < HEAD
    first_two = (iota((length, 2 * PAIR), 1) & HEAD) == 0
    first_tall = iota((2 * length, PAIR), 1) < HEAD
    pairs = q_ref.shape[1] // PAIR
    stage = []
    for p in range(pairs):
        span = slice(p * PAIR, (p + 1) * PAIR)
        q = q_ref[:, span].astype(F32)
        k = k_ref[:, span].astype(F32)
        v = v_ref[:, span]
        log_decay = decays[:, span]
        squares = dot(lanes(*split(k * k)), ones_twice)
        unit = k * lax.rsqrt(1.0 + squares)
        erase = unit * rates[:, span]
        running = dot(lower_twice, rows(*split(log_decay)))
        before = running - log_decay
        centre = running[length // 2 : length // 2 + 1]
        final = running[length - 1 :]
        back = jnp.exp(centre - running)
        centre_decay = jnp.exp(centre)
        rest_decay = jnp.exp(final - centre)
        erase_from = unit * jnp.exp(before - centre)
        read_mid = q * jnp.exp(running - centre)
        key_to = k * back
        erase_to = erase * back
        left = rows(erase_from, read_mid)
        right = rows(key_to, erase_to)
        left_high, left_low = split(left)
        left_low_turned = half_turn(left - left_high.astype(F32)).astype(BF16)
        right_high, right_low = split(right)
        right_turned = half_turn(right).astype(BF16)
        nothing = jnp.zeros_like(right_high)
        v_twice = rows(v, v)
        heads = []
        for own in (first_tall, ~first_tall):
            pairings = dot_nt(
                lanes(jnp.where(own, left_high, left_low_turned), left_high),
                lanes(jnp.where(own, right_high, right_turned), jnp.where(own, right_low, nothing)),
            )
            key_pairs = jnp.where(strict, pairings[:length, :length], 0.0)
            erase_pairs = jnp.where(strict, pairings[:length, length:], 0.0)
            read_keys = jnp.where(within, pairings[length:, :length], 0.0)
            read_erase = jnp.where(within, pairings[length:, length:], 0.0)
            applied = dot(lanes(*split(rows(key_pairs, read_keys))), v_twice)
            heads.append((erase_pairs, split(read_erase), applied))
        applied = jnp.where(first_tall, heads[0][2], heads[1][2])
        stage.append(
            dict(
                heads=heads,
                sides=lanes(erase_from * centre_decay, applied[:length]),
                own_read=applied[length:],
                read_start=read_mid * centre_decay,
                key_end=key_to * rest_decay,
                erase_end=erase_to * rest_decay,
                keep=jnp.exp(final) - 1.0,
                v_twice=v_twice,
            )
        )
    solved = inverses([h[0] for s in stage for h in s["heads"]], length)
    for p in range(pairs):
        s = stage[p]
        span = slice(p * PAIR, (p + 1) * PAIR)
        sides = split(s["sides"])
        inner = jnp.where(first_two, product(solved[2 * p], sides), product(solved[2 * p + 1], sides))
        inner = split(inner)
        taken = jnp.where(
            first_two, product(s["heads"][0][1], inner), product(s["heads"][1][1], inner)
        )
        r_ref[:, span] = s["read_start"] - taken[:, :PAIR]
        o_ref[:, span] = s["own_read"] - taken[:, PAIR:]
        ended = product(split(s["erase_end"].T), inner)
        gained = dot(lanes(*split(s["key_end"].T)), s["v_twice"])
        transfer = jnp.where(row == col, s["keep"], 0.0) - ended[:, :PAIR]
        added = gained - ended[:, PAIR:]
        msg_ref[2 * p] = jnp.where(first, transfer, half_turn(added))[:HEAD].astype(BF16)
        msg_ref[2 * p + 1] = jnp.where(first, half_turn(transfer), added)[HEAD:].astype(BF16)


def scan_kernel(msg_ref, start_ref):
    first = iota((HEAD, PAIR), 1) < HEAD
    eye = (iota((HEAD, PAIR), 0) + HEAD == iota((HEAD, PAIR), 1)).astype(F32).astype(BF16)
    nothing = jnp.zeros((HEAD, PAIR), BF16)
    state = jnp.zeros((HEAD, PAIR), F32)
    chunks = msg_ref.shape[0]
    half = HEAD // 2
    for i in range(chunks):
        start_ref[i] = jnp.where(first[:half], state[:half], state[half:]).astype(BF16)
        if i + 1 < chunks:
            high, low = split(state)
            left = lanes(jnp.where(first, high, eye), jnp.where(first, low, nothing))
            here = msg_ref[i]
            here = rows(here, here)
            state = state + dot_nt(left, lanes(here, here))


def finish_kernel(start_ref, r_ref, o_ref, gain_ref, w_ref, out_ref, mix_ref):
    length = r_ref.shape[0]

    @pl.when(pl.program_id(0) == 0)
    def _():
        ones = same_head()
        ones_twice = rows(ones, ones)
        half = HEAD // 2
        first = iota((half, PAIR), 1) < HEAD
        for p in range(r_ref.shape[1] // PAIR):
            span = slice(p * PAIR, (p + 1) * PAIR)
            one = start_ref[2 * p].astype(F32)
            two = start_ref[2 * p + 1].astype(F32)
            states = rows(
                jnp.where(first, one, 0.0),
                jnp.where(first, half_turn(one), 0.0),
                jnp.where(first, 0.0, half_turn(two)),
                jnp.where(first, 0.0, two),
            ).astype(BF16)
            readout = o_ref[:, span] + dot_nt(lanes(*split(r_ref[:, span])), lanes(states, states))
            average = dot(lanes(*split(readout)), ones_twice) * (1.0 / HEAD)
            centred = readout - average
            variance = dot(lanes(*split(centred * centred)), ones_twice) * (1.0 / HEAD)
            normed = centred * lax.rsqrt(variance + 1.0)
            mix_ref[:, span] = (normed * gain_ref[:, span]).astype(BF16)

    out_ref[...] = dot(mix_ref[...], w_ref[0]).astype(BF16)


def local_chunk(q, k, v, dl, rl, du, ru, base):
    length, width = q.shape
    heads = width // HEAD
    step = GROUP * HEAD
    wide = pl.BlockSpec((length, step), lambda i: (0, i))
    low = pl.BlockSpec(dl.shape, lambda i: (0, 0))
    up = pl.BlockSpec((du.shape[0], step), lambda i: (0, i))
    return pl.pallas_call(
        local_kernel,
        grid=(width // step,),
        in_specs=[wide, wide, wide, low, low, up, up, pl.BlockSpec((1, step), lambda i: (0, i))],
        out_specs=[pl.BlockSpec((GROUP, HEAD, PAIR), lambda i: (i, 0, 0)), wide, wide],
        out_shape=[
            jax.ShapeDtypeStruct((heads, HEAD, PAIR), BF16),
            jax.ShapeDtypeStruct((length, width), F32),
            jax.ShapeDtypeStruct((length, width), F32),
        ],
        name="local_chunk",
    )(q, k, v, dl, rl, du, ru, base.reshape(1, width))


def scan_chunks(msg):
    chunks = msg.shape[0]
    return pl.pallas_call(
        scan_kernel,
        out_shape=jax.ShapeDtypeStruct((chunks, HEAD // 2, PAIR), BF16),
        name="scan_chunks",
    )(msg)


def finish(starts, r, o, gain, weight):
    length, width = r.shape
    parts, _, cols = weight.shape
    whole = lambda a: pl.BlockSpec(a.shape, lambda j: (0,) * a.ndim)
    gain = gain.reshape(1, width)
    return pl.pallas_call(
        finish_kernel,
        grid=(parts,),
        in_specs=[
            whole(starts),
            whole(r),
            whole(o),
            whole(gain),
            pl.BlockSpec((1, width, cols), lambda j: ((j % 2) * (parts // 2) + j // 2, 0, 0)),
        ],
        out_specs=pl.BlockSpec((length, cols), lambda j: (0, j)),
        out_shape=jax.ShapeDtypeStruct((length, parts * cols), BF16),
        scratch_shapes=[pltpu.VMEM((length, width), BF16)],
        name="finish",
    )(starts, r, o, gain, weight)


def per_device(
    query_rows, key_rows, value_rows, decay_low, rate_low, decay_up, rate_up, decay_base, norm_gain, out_weight
):
    columns = lax.all_gather(lax.all_gather(out_weight, "dp_0"), "dp_1")
    columns = columns.reshape(-1, *out_weight.shape)
    msg, r, o = local_chunk(
        query_rows[0], key_rows[0], value_rows[0], decay_low[0], rate_low[0], decay_up, rate_up, decay_base
    )
    here = lax.all_to_all(msg, "sp", split_axis=0, concat_axis=0, tiled=True)
    starts = scan_chunks(here)
    back = lax.all_to_all(starts, "sp", split_axis=0, concat_axis=0, tiled=True)
    return finish(back, r, o, norm_gain, columns)[None]


def solution(mesh):
    split_mesh = Mesh(mesh.devices.reshape(mesh.shape["sp"], 8, 2), ("sp", "dp_0", "dp_1"))
    placed = (
        P(DP, "sp", None),
        P(DP, "sp", None),
        P(DP, "sp", None),
        P(DP, "sp", None),
        P(DP, "sp", None),
        P(),
        P(),
        P(),
        P(),
        P(None, DP),
    )
    return jax.shard_map(
        per_device, mesh=split_mesh, in_specs=placed, out_specs=P(DP, "sp", None), check_vma=False
    )
```

profile of v0, /device:TPU:1, one launch (start us, length us, event | category | flops | bytes accessed | tf_op | source)
XLA Modules:
  0.0 181.0 jit_solution(6400039027939807344)
XLA Ops:
  6.5 0.0 all-gather.5.cloned.1.call-start
  6.5 0.7 all-gather.5.cloned.1.call-update
  7.3 0.0 all-gather.7.cloned.1.call-start
  7.3 64.5 %all-gather.5.cloned.1.call-done = bf16[16384,128]{1,0:T(8,128)(2,1)} async-done(((bf16[2048,128]{1,0:T(8,128)(2,1)}), bf16[16384,128]{1,0:T(8,128)(2,1)}) %all-gather.5.cloned.1.call-update) | async-done | bytes 4194320 | tf_op jit(solution)/shard_map/all_gather | solution.py:272
  71.8 0.0 all-gather.7.cloned.1.call-update
  71.8 38.7 %local_chunk.1 = (bf16[32,64,128]{2,1,0:T(8,128)(2,1)}, f32[128,2048]{1,0:T(8,128)}, f32[128,2048]{1,0:T(8,128)}) custom-call(bf16[128,2048]{1,0:T(8,128)(2,1)} %bitcast.10, bf16[128,2048]{1,0:T(8,128)(2,1)} %bitcast.11, bf16[128,2048]{1,0:T(8,128)(2,1)} %bitcast.12, bf16[128,128]{1,0:T(8,128)(2,1)} %bitcast.13, bf16[128,128]{1,0:T(8,128)(2,1)} %bitcast.14, ...), custom_call_target="tpu_custom_call" | custom-call | tf_op jit(solution)/shard_map/local_chunk/pallas_call | solution.py:224
  110.6 25.6 %all_to_all.10.msg_ref = bf16[32,64,128]{2,1,0:T(8,128)(2,1)} all-to-all(bf16[32,64,128]{2,1,0:T(8,128)(2,1)} %get-tuple-element.8), channel_id=1, replica_groups=mesh['sp'=32,'dp_0'=8,'dp_1'=2] {'sp'}, dimensions={0} | all-to-all | bytes 1048576 | tf_op jit(solution)/shard_map/all_to_all | solution.py:277
  136.2 5.5 %scan_chunks.1 = bf16[32,32,128]{2,1,0:T(8,128)(2,1)} custom-call(bf16[32,64,128]{2,1,0:T(8,128)(2,1)} %all_to_all.10.msg_ref), custom_call_target="tpu_custom_call" | custom-call | tf_op jit(solution)/shard_map/scan_chunks/pallas_call | solution.py:240
  141.7 16.5 %all_to_all.11.start_ref = bf16[32,32,128]{2,1,0:T(8,128)(2,1)} all-to-all(bf16[32,32,128]{2,1,0:T(8,128)(2,1)} %scan_chunks.1), channel_id=1, replica_groups=mesh['sp'=32,'dp_0'=8,'dp_1'=2] {'sp'}, dimensions={0} | all-to-all | bytes 524288 | tf_op jit(solution)/shard_map/all_to_all | solution.py:279
  158.2 0.0 all-gather.7.cloned.1.call-done.w_ref
  158.2 16.0 %finish.1 = bf16[128,2048]{1,0:T(8,128)(2,1)} custom-call(bf16[32,32,128]{2,1,0:T(8,128)(2,1)} %all_to_all.11.start_ref, f32[128,2048]{1,0:T(8,128)} %get-tuple-element.9.r_ref, f32[128,2048]{1,0:T(8,128)} %get-tuple-element.10.o_ref, f32[1,2048]{1,0:T(1,128)} %bitcast.16, bf16[16,2048,128]{2,1,0:T(8,128)(2,1)} %all-gather.7.cloned.1.call-done.w_ref), custom_call_target="tpu_custom_call" | custom-call | tf_op jit(solution)/shard_map/finish/pallas_call | solution.py:252
Async XLA Ops:
  6.5 65.3 %all-gather.5.cloned.1.call-start = ((), (), s32[]{:S(2)}) async-start(), calls=%async_computation.2 | async-start | bytes 4718592 | tf_op jit(solution)/shard_map/all_gather | solution.py:272
  7.3 150.9 %all-gather.7.cloned.1.call-start = ((), (), s32[]{:S(2)}) async-start(), calls=%async_computation.3 | async-start | bytes 12582912 | tf_op jit(solution)/shard_map/all_gather | solution.py:272
Sparse Core Ops, SparseCore 0:
  9.4 62.3 all-gather.4
  73.9 28.6 all-gather.6
where the time goes:
time: 183 us; the launch traced here: 181 us
  waiting for transfers between devices  65.2 us (36%)
  Pallas kernels  60.2 us (33%)
  blocking collectives  42.1 us (23%)
  between operations  13.4 us (7%)
    all_gather x2, waiting for transfers between devices, per_device(): columns = lax.all_gather(lax.all_gather(out_weight, 'dp_0'), 'dp_1')  64.5 us
    pallas_call x1, Pallas kernels, local_chunk(): pl.pallas_call(local_kernel, grid=(width // step,), in_specs=[wide, wide,...  38.7 us
    all_to_all x1, blocking collectives, per_device(): here = lax.all_to_all(msg, 'sp', split_axis=0, concat_axis=0, tiled=True)  25.6 us
    all_to_all x1, blocking collectives, per_device(): back = lax.all_to_all(starts, 'sp', split_axis=0, concat_axis=0, tiled=True)  16.5 us
    pallas_call x1, Pallas kernels, finish(): pl.pallas_call(finish_kernel, grid=(parts,), in_specs=[whole(starts), who...  16 us
    pallas_call x1, Pallas kernels, scan_chunks(): pl.pallas_call(scan_kernel, out_shape=jax.ShapeDtypeStruct((chunks, HEAD...  5.51 us
  transfers between devices with their start and end apart: 2, of which 1 were waited for; matrix products, arithmetic and copies ran while one was open for 0% of the time, Pallas kernels for 24%

commit v1 on v0

--- a/solution.py
+++ b/solution.py
@@ -41,9 +41,13 @@
 
 
 def product(left, right):
-    left_high, left_low = left
+    left = lanes(*left)
     right_high, right_low = right
-    return dot(lanes(left_high, left_low), rows(right_high, right_high)) + dot(left_high, right_low)
+    if right_high.shape[1] > PAIR:
+        return dot(left, rows(right_high, right_high)) + dot(left, rows(right_low, right_low))
+    both = lanes(right_high, right_low)
+    both = dot(left, rows(both, both))
+    return both[:, :PAIR] + both[:, PAIR:]
 
 
 def iota(shape, dim):
@@ -63,19 +67,35 @@
     solved = [eye - jnp.where(apart == 1, m, 0.0) for m in matrices]
     block = 2
     while block < length:
-        here = (apart >= block) & (apart < 2 * block)
+        here = ((apart >= block) & (apart < 2 * block)).astype(F32).astype(BF16)
         parts = [split(s) for s in solved]
-        masked = [
-            (jnp.where(here, h, jnp.zeros_like(h)), jnp.where(here, l, jnp.zeros_like(l)))
-            for h, l in pieces
-        ]
-        inner = [split(product(c, x)) for c, x in zip(masked, parts)]
-        solved = [s - product(x, d) for s, x, d in zip(solved, parts, inner)]
+        if block < 16:
+            inner = [split(product((h * here, l * here), x)) for (h, l), x in zip(pieces, parts)]
+            solved = [s - product(x, d) for s, x, d in zip(solved, parts, inner)]
+        else:
+            spans = range(0, length, 2 * block)
+            odd = lambda m: rows(*(m[at + block : at + 2 * block] for at in spans))
+            here = odd(here)
+            gap = jnp.zeros((block, length), BF16)
+            spread = lambda m: rows(*(x for i in range(len(spans)) for x in (gap, m[i * block : (i + 1) * block])))
+            inner = [split(product((odd(h) * here, odd(l) * here), x)) for (h, l), x in zip(pieces, parts)]
+            taken = [product((odd(h), odd(l)), (spread(dh), spread(dl))) for (h, l), (dh, dl) in zip(parts, inner)]
+            solved = [
+                rows(
+                    *(
+                        x
+                        for i, at in enumerate(spans)
+                        for x in (s[at : at + block], s[at + block : at + 2 * block] - t[i * block : (i + 1) * block])
+                    )
+                )
+                for s, t in zip(solved, taken)
+            ]
         block *= 2
     return [split(s) for s in solved]
 
 
-def local_kernel(q_ref, k_ref, v_ref, dl_ref, rl_ref, du_ref, ru_ref, base_ref, msg_ref, r_ref, o_ref):
+def local_kernel(q_ref, k_ref, v_ref, dl_ref, rl_ref, du_ref, ru_ref, base_ref, *outs):
+    msg_ref, erase_ref, inner_ref, read_ref, own_ref = outs
     length = q_ref.shape[0]
     row = iota((length, length), 0)
     col = iota((length, length), 1)
@@ -155,11 +175,12 @@
         sides = split(s["sides"])
         inner = jnp.where(first_two, product(solved[2 * p], sides), product(solved[2 * p + 1], sides))
         inner = split(inner)
-        taken = jnp.where(
-            first_two, product(s["heads"][0][1], inner), product(s["heads"][1][1], inner)
-        )
-        r_ref[:, span] = s["read_start"] - taken[:, :PAIR]
-        o_ref[:, span] = s["own_read"] - taken[:, PAIR:]
+        for part in range(2):
+            inner_ref[p, part] = inner[part]
+            erase_ref[2 * p, part] = s["heads"][0][1][part]
+            erase_ref[2 * p + 1, part] = s["heads"][1][1][part]
+        read_ref[:, span] = s["read_start"]
+        own_ref[:, span] = s["own_read"]
         ended = product(split(s["erase_end"].T), inner)
         gained = dot(lanes(*split(s["key_end"].T)), s["v_twice"])
         transfer = jnp.where(row == col, s["keep"], 0.0) - ended[:, :PAIR]
@@ -168,7 +189,18 @@
         msg_ref[2 * p + 1] = jnp.where(first, half_turn(transfer), added)[HEAD:].astype(BF16)
 
 
-def scan_kernel(msg_ref, start_ref):
+def adjust_kernel(base_ref, erase_ref, inner_ref, out_ref):
+    length = base_ref.shape[0]
+    first = iota((length, PAIR), 1) < HEAD
+    for p in range(base_ref.shape[1] // PAIR):
+        span = slice(p * PAIR, (p + 1) * PAIR)
+        inner = (inner_ref[p, 0], inner_ref[p, 1])
+        one = product((erase_ref[2 * p, 0], erase_ref[2 * p, 1]), inner)
+        two = product((erase_ref[2 * p + 1, 0], erase_ref[2 * p + 1, 1]), inner)
+        out_ref[:, span] = base_ref[:, span] - jnp.where(first, one, two)
+
+
+def scan_kernel(msg_ref, after_ref, start_ref):
     first = iota((HEAD, PAIR), 1) < HEAD
     eye = (iota((HEAD, PAIR), 0) + HEAD == iota((HEAD, PAIR), 1)).astype(F32).astype(BF16)
     nothing = jnp.zeros((HEAD, PAIR), BF16)
@@ -185,33 +217,47 @@
             state = state + dot_nt(left, lanes(here, here))
 
 
-def finish_kernel(start_ref, r_ref, o_ref, gain_ref, w_ref, out_ref, mix_ref):
-    length = r_ref.shape[0]
-
-    @pl.when(pl.program_id(0) == 0)
-    def _():
-        ones = same_head()
-        ones_twice = rows(ones, ones)
-        half = HEAD // 2
-        first = iota((half, PAIR), 1) < HEAD
-        for p in range(r_ref.shape[1] // PAIR):
-            span = slice(p * PAIR, (p + 1) * PAIR)
-            one = start_ref[2 * p].astype(F32)
-            two = start_ref[2 * p + 1].astype(F32)
-            states = rows(
-                jnp.where(first, one, 0.0),
-                jnp.where(first, half_turn(one), 0.0),
-                jnp.where(first, 0.0, half_turn(two)),
-                jnp.where(first, 0.0, two),
-            ).astype(BF16)
-            readout = o_ref[:, span] + dot_nt(lanes(*split(r_ref[:, span])), lanes(states, states))
-            average = dot(lanes(*split(readout)), ones_twice) * (1.0 / HEAD)
-            centred = readout - average
-            variance = dot(lanes(*split(centred * centred)), ones_twice) * (1.0 / HEAD)
-            normed = centred * lax.rsqrt(variance + 1.0)
-            mix_ref[:, span] = (normed * gain_ref[:, span]).astype(BF16)
-
-    out_ref[...] = dot(mix_ref[...], w_ref[0]).astype(BF16)
+def finish_kernel(start_ref, r_ref, o_ref, gain_ref, w_ref, out_ref, mix_ref, here_ref, done_ref):
+    copies = [pltpu.make_async_copy(w_ref.at[k], here_ref.at[k], done_ref.at[k]) for k in range(w_ref.shape[0])]
+    for copy in copies:
+        copy.start()
+    width = r_ref.shape[1]
+    ones = same_head()
+    ones_twice = rows(ones, ones)
+    half = HEAD // 2
+    first = iota((half, PAIR), 1) < HEAD
+    for p in range(width // PAIR):
+        span = slice(p * PAIR, (p + 1) * PAIR)
+        one = start_ref[2 * p].astype(F32)
+        two = start_ref[2 * p + 1].astype(F32)
+        states = rows(
+            jnp.where(first, one, 0.0),
+            jnp.where(first, half_turn(one), 0.0),
+            jnp.where(first, 0.0, half_turn(two)),
+            jnp.where(first, 0.0, two),
+        ).astype(BF16)
+        readout = o_ref[:, span] + dot_nt(lanes(*split(r_ref[:, span])), lanes(states, states))
+        average = dot(lanes(*split(readout)), ones_twice) * (1.0 / HEAD)
+        centred = readout - average
+        variance = dot(lanes(*split(centred * centred)), ones_twice) * (1.0 / HEAD)
+        normed = centred * lax.rsqrt(variance + 1.0)
+        mix_ref[:, span] = (normed * gain_ref[:, span]).astype(BF16)
+
+    mix = mix_ref[...]
+    for k in range(0, w_ref.shape[0], 2):
+        copies[k].wait()
+        copies[k + 1].wait()
+        out_ref[:, k * 128 : (k + 2) * 128] = dot(mix, lanes(here_ref[k], here_ref[k + 1])).astype(BF16)
+
+
+FLOPS_PER_US = 500_000_000
+
+
+def budget(mib, us):
+    return dict(
+        compiler_params=pltpu.CompilerParams(vmem_limit_bytes=mib << 20),
+        cost_estimate=pl.CostEstimate(flops=int(us * FLOPS_PER_US), transcendentals=0, bytes_accessed=1 << 20),
+    )
 
 
 def local_chunk(q, k, v, dl, rl, du, ru, base):
@@ -221,62 +267,89 @@
     wide = pl.BlockSpec((length, step), lambda i: (0, i))
     low = pl.BlockSpec(dl.shape, lambda i: (0, 0))
     up = pl.BlockSpec((du.shape[0], step), lambda i: (0, i))
+    bias = pl.BlockSpec((1, step), lambda i: (0, i))
     return pl.pallas_call(
         local_kernel,
         grid=(width // step,),
-        in_specs=[wide, wide, wide, low, low, up, up, pl.BlockSpec((1, step), lambda i: (0, i))],
-        out_specs=[pl.BlockSpec((GROUP, HEAD, PAIR), lambda i: (i, 0, 0)), wide, wide],
+        in_specs=[wide, wide, wide, low, low, up, up, bias],
+        out_specs=[
+            pl.BlockSpec((GROUP, HEAD, PAIR), lambda i: (i, 0, 0)),
+            pl.BlockSpec((GROUP, 2, length, length), lambda i: (i, 0, 0, 0)),
+            pl.BlockSpec((GROUP // 2, 2, length, 2 * PAIR), lambda i: (i, 0, 0, 0)),
+            wide,
+            wide,
+        ],
         out_shape=[
             jax.ShapeDtypeStruct((heads, HEAD, PAIR), BF16),
+            jax.ShapeDtypeStruct((heads, 2, length, length), BF16),
+            jax.ShapeDtypeStruct((heads // 2, 2, length, 2 * PAIR), BF16),
             jax.ShapeDtypeStruct((length, width), F32),
             jax.ShapeDtypeStruct((length, width), F32),
         ],
         name="local_chunk",
+        **budget(60, 35),
     )(q, k, v, dl, rl, du, ru, base.reshape(1, width))
 
 
-def scan_chunks(msg):
+def adjust(start, erase, inner, half):
+    length, width = start.shape
+    count = 2 * GROUP
+    step = count * HEAD
+    wide = pl.BlockSpec((length, step), lambda i: (0, i))
+    return pl.pallas_call(
+        adjust_kernel,
+        grid=(width // step,),
+        in_specs=[
+            wide,
+            pl.BlockSpec((count, 2, length, length), lambda i: (i, 0, 0, 0)),
+            pl.BlockSpec((count // 2, 2, length, PAIR), lambda i: (i, 0, 0, half)),
+        ],
+        out_specs=wide,
+        out_shape=jax.ShapeDtypeStruct((length, width), F32),
+        name="adjust",
+        **budget(60, 3),
+    )(start, erase, inner)
+
+
+def scan_chunks(msg, after):
     chunks = msg.shape[0]
     return pl.pallas_call(
         scan_kernel,
+        in_specs=[pl.BlockSpec(memory_space=pltpu.VMEM), pl.BlockSpec(memory_space=pltpu.HBM)],
         out_shape=jax.ShapeDtypeStruct((chunks, HEAD // 2, PAIR), BF16),
         name="scan_chunks",
-    )(msg)
+        **budget(4, 6),
+    )(msg, after)
 
 
 def finish(starts, r, o, gain, weight):
     length, width = r.shape
-    parts, _, cols = weight.shape
-    whole = lambda a: pl.BlockSpec(a.shape, lambda j: (0,) * a.ndim)
-    gain = gain.reshape(1, width)
     return pl.pallas_call(
         finish_kernel,
-        grid=(parts,),
-        in_specs=[
-            whole(starts),
-            whole(r),
-            whole(o),
-            whole(gain),
-            pl.BlockSpec((1, width, cols), lambda j: ((j % 2) * (parts // 2) + j // 2, 0, 0)),
+        in_specs=[pl.BlockSpec(memory_space=pltpu.VMEM)] * 4 + [pl.BlockSpec(memory_space=pltpu.HBM)],
+        out_shape=jax.ShapeDtypeStruct((length, weight.shape[0] * weight.shape[2]), BF16),
+        scratch_shapes=[
+            pltpu.VMEM((length, width), BF16),
+            pltpu.VMEM(weight.shape, BF16),
+            pltpu.SemaphoreType.DMA((weight.shape[0],)),
         ],
-        out_specs=pl.BlockSpec((length, cols), lambda j: (0, j)),
-        out_shape=jax.ShapeDtypeStruct((length, parts * cols), BF16),
-        scratch_shapes=[pltpu.VMEM((length, width), BF16)],
         name="finish",
-    )(starts, r, o, gain, weight)
+        **budget(40, 12),
+    )(starts, r, o, gain.reshape(1, width), weight)
 
 
 def per_device(
     query_rows, key_rows, value_rows, decay_low, rate_low, decay_up, rate_up, decay_base, norm_gain, out_weight
 ):
-    columns = lax.all_gather(lax.all_gather(out_weight, "dp_0"), "dp_1")
-    columns = columns.reshape(-1, *out_weight.shape)
-    msg, r, o = local_chunk(
+    columns = lax.all_gather(out_weight, DP)
+    msg, erase, inner, read, own_read = local_chunk(
         query_rows[0], key_rows[0], value_rows[0], decay_low[0], rate_low[0], decay_up, rate_up, decay_base
     )
     here = lax.all_to_all(msg, "sp", split_axis=0, concat_axis=0, tiled=True)
-    starts = scan_chunks(here)
+    r = adjust(read, erase, inner, 0)
+    starts = scan_chunks(here, r)
     back = lax.all_to_all(starts, "sp", split_axis=0, concat_axis=0, tiled=True)
+    o = adjust(own_read, erase, inner, 1)
     return finish(back, r, o, norm_gain, columns)[None]
 
 

time: 183 us -> 117 us (0.64)
  the two profiles are of different devices: /device:TPU:1 before, /device:TPU:8 now
where the time goes in v1:
time: 117 us; the launch traced here: 116 us
  Pallas kernels  57.7 us (49%)
  waiting for transfers between devices  21.6 us (18%)
  starting transfers between devices  17.8 us (15%)
  between operations  13.5 us (12%)
  local copies, waits for them, and re-layouts  5.84 us (5%)
    pallas_call x1, Pallas kernels, local_chunk(): pl.pallas_call(local_kernel, grid=(width // step,), in_specs=[wide, wide,...  36.2 us
    all_to_all x1, waiting for transfers between devices, per_device(): here = lax.all_to_all(msg, 'sp', split_axis=0, concat_axis=0, tiled=True)  13.2 us
    all_to_all x1, starting transfers between devices, per_device(): here = lax.all_to_all(msg, 'sp', split_axis=0, concat_axis=0, tiled=True)  13.2 us
    pallas_call x2, Pallas kernels, adjust(): pl.pallas_call(adjust_kernel, grid=(width // step,), in_specs=[wide, pl.B...  9.18 us
    pallas_call x1, Pallas kernels, finish(): pl.pallas_call(finish_kernel, in_specs=[pl.BlockSpec(memory_space=pltpu.V...  7.87 us
    all_to_all x1, waiting for transfers between devices, per_device(): back = lax.all_to_all(starts, 'sp', split_axis=0, concat_axis=0, tiled=True)  7.69 us
    unnamed x10, local copies, waits for them, and re-layouts  5.84 us
    all_to_all x1, starting transfers between devices, per_device(): back = lax.all_to_all(starts, 'sp', split_axis=0, concat_axis=0, tiled=True)  4.67 us
  transfers between devices with their start and end apart: 3, of which 2 were waited for; matrix products, arithmetic and copies ran while one was open for 0% of the time, Pallas kernels for 43%

profile of v1, /device:TPU:8, one launch (start us, length us, event | category | flops | bytes accessed | tf_op | source)
XLA Modules:
  0.0 116.4 jit_solution(15945493439667562429)
XLA Ops:
  6.5 0.0 all-gather.3.cloned.1.call-start
  6.5 0.7 all-gather.3.cloned.1.call-update
  7.3 36.2 %local_chunk.1 = (bf16[32,64,128]{2,1,0:T(8,128)(2,1)}, bf16[32,2,128,128]{3,2,1,0:T(8,128)(2,1)}, bf16[16,2,128,256]{3,2,1,0:T(8,128)(2,1)}, f32[128,2048]{1,0:T(8,128)}, f32[128,2048]{1,0:T(8,128)}) custom-call(bf16[128,2048]{1,0:T(8,128)(2,1)} %bitcast.11, bf16[128,2048]{1,0:T(8,128)(2,1)} %bitcast.12, bf16[128,2048]{1,0:T(8,128)(2,1)} %bitcast.13, ...), custom_call_target="tpu_custom_call" | custom-call | flops 17500000256 | bytes 1048576 | tf_op jit(solution)/shard_map/local_chunk/pallas_call | solution.py:271
  43.4 13.2 %all-to-all-start = ((bf16[32,64,128]{2,1,0:T(8,128)(2,1)}), bf16[32,64,128]{2,1,0:T(8,128)(2,1)S(1)}, u32[]{:S(2)}, u32[]{:S(2)}) async-start(bf16[32,64,128]{2,1,0:T(8,128)(2,1)} %get-tuple-element.10), calls=%async_computation | async-start | bytes 1048576 | tf_op jit(solution)/shard_map/all_to_all | solution.py:348
  56.6 4.5 %adjust.2.after_ref.r_ref = f32[128,2048]{1,0:T(8,128)} custom-call(f32[128,2048]{1,0:T(8,128)} %get-tuple-element.11.base_ref, bf16[32,2,128,128]{3,2,1,0:T(8,128)(2,1)} %get-tuple-element.12.erase_ref, bf16[16,2,128,256]{3,2,1,0:T(8,128)(2,1)} %get-tuple-element.13.inner_ref), custom_call_target="tpu_custom_call" | custom-call | flops 1500000000 | bytes 1048576 | tf_op jit(solution)/shard_map/adjust/pallas_call | solution.py:299
  61.2 13.2 %all-to-all-done.msg_ref = bf16[32,64,128]{2,1,0:T(8,128)(2,1)S(1)} async-done(((bf16[32,64,128]{2,1,0:T(8,128)(2,1)}), bf16[32,64,128]{2,1,0:T(8,128)(2,1)S(1)}, u32[]{:S(2)}, u32[]{:S(2)}) %all-to-all-start) | async-done | bytes 524320 | tf_op jit(solution)/shard_map/all_to_all | solution.py:348
  74.4 0.0 copy-start
  74.4 1.2 %copy-done = f32[128,2048]{1,0:T(8,128)S(1)} copy-done((f32[128,2048]{1,0:T(8,128)S(1)}, f32[128,2048]{1,0:T(8,128)}, u32[]{:S(2)}) %copy-start) | copy-done | bytes 1048600
  75.6 4.5 %scan_chunks.1 = bf16[32,32,128]{2,1,0:T(8,128)(2,1)} custom-call(bf16[32,64,128]{2,1,0:T(8,128)(2,1)S(1)} %all-to-all-done.msg_ref, f32[128,2048]{1,0:T(8,128)S(1)} %copy-done), custom_call_target="tpu_custom_call" | custom-call | flops 3000000000 | bytes 1048576 | tf_op jit(solution)/shard_map/scan_chunks/pallas_call | solution.py:316
  80.0 4.7 %all-to-all-start.1 = ((bf16[32,32,128]{2,1,0:T(8,128)(2,1)}), bf16[32,32,128]{2,1,0:T(8,128)(2,1)S(1)}, u32[]{:S(2)}, u32[]{:S(2)}) async-start(bf16[32,32,128]{2,1,0:T(8,128)(2,1)} %scan_chunks.1), calls=%async_computation.1 | async-start | bytes 524288 | tf_op jit(solution)/shard_map/all_to_all | solution.py:351
  84.7 0.0 copy-start.1
  84.7 0.0 copy-start.4
  84.7 4.6 %adjust.3.o_ref = f32[128,2048]{1,0:T(8,128)} custom-call(f32[128,2048]{1,0:T(8,128)} %get-tuple-element.14.base_ref, bf16[32,2,128,128]{3,2,1,0:T(8,128)(2,1)} %get-tuple-element.12.erase_ref, bf16[16,2,128,256]{3,2,1,0:T(8,128)(2,1)} %get-tuple-element.13.inner_ref), custom_call_target="tpu_custom_call" | custom-call | flops 1500000000 | bytes 1048576 | tf_op jit(solution)/shard_map/adjust/pallas_call | solution.py:299
  89.4 7.7 %all-to-all-done.1.start_ref = bf16[32,32,128]{2,1,0:T(8,128)(2,1)S(1)} async-done(((bf16[32,32,128]{2,1,0:T(8,128)(2,1)}), bf16[32,32,128]{2,1,0:T(8,128)(2,1)S(1)}, u32[]{:S(2)}, u32[]{:S(2)}) %all-to-all-start.1) | async-done | bytes 262176 | tf_op jit(solution)/shard_map/all_to_all | solution.py:351
  97.1 0.0 all-gather.3.cloned.1.call-done
  97.1 0.0 copy-done.1
  97.1 0.0 copy-done.4
  97.1 0.0 copy-start.2
  97.1 1.2 %copy-done.2 = f32[128,2048]{1,0:T(8,128)S(1)} copy-done((f32[128,2048]{1,0:T(8,128)S(1)}, f32[128,2048]{1,0:T(8,128)}, u32[]{:S(2)}) %copy-start.2) | copy-done | bytes 1048600
  98.3 0.0 copy-start.3
  98.3 3.4 %copy-done.3 = bf16[32768,128]{1,0:T(8,128)(2,1)S(1)} copy-done((bf16[32768,128]{1,0:T(8,128)(2,1)S(1)}, bf16[32768,128]{1,0:T(8,128)(2,1)}, u32[]{:S(2)}) %copy-start.3) | copy-done | bytes 8388632
  101.7 7.9 %finish.1 = bf16[128,2048]{1,0:T(8,128)(2,1)} custom-call(bf16[32,32,128]{2,1,0:T(8,128)(2,1)S(1)} %all-to-all-done.1.start_ref, f32[128,2048]{1,0:T(8,128)S(1)} %copy-done.1, f32[128,2048]{1,0:T(8,128)S(1)} %copy-done.2, f32[1,2048]{1,0:T(1,128)S(1)} %bitcast.10, bf16[16,2048,128]{2,1,0:T(8,128)(2,1)S(1)} %bitcast.9), custom_call_target="tpu_custom_call" | custom-call | flops 6000000000 | bytes 1048576 | tf_op jit(solution)/shard_map/finish/pallas_call | solution.py:327
Async XLA Ops:
  6.5 90.5 %all-gather.3.cloned.1.call-start = ((), (), s32[]{:S(2)}) async-start(), calls=%async_computation.2 | async-start | bytes 8912896 | tf_op jit(solution)/shard_map/all_gather | solution.py:344
  43.4 30.9 %all-to-all-start = ((bf16[32,64,128]{2,1,0:T(8,128)(2,1)}), bf16[32,64,128]{2,1,0:T(8,128)(2,1)S(1)}, u32[]{:S(2)}, u32[]{:S(2)}) async-start(bf16[32,64,128]{2,1,0:T(8,128)(2,1)} %get-tuple-element.10), calls=%async_computation | async-start | bytes 1048576 | tf_op jit(solution)/shard_map/all_to_all | solution.py:348
  74.4 1.2 %copy-start = (f32[128,2048]{1,0:T(8,128)S(1)}, f32[128,2048]{1,0:T(8,128)}, u32[]{:S(2)}) copy-start(f32[128,2048]{1,0:T(8,128)} %adjust.2.after_ref.r_ref) | copy-start | bytes 3145732
  80.0 17.0 %all-to-all-start.1 = ((bf16[32,32,128]{2,1,0:T(8,128)(2,1)}), bf16[32,32,128]{2,1,0:T(8,128)(2,1)S(1)}, u32[]{:S(2)}, u32[]{:S(2)}) async-start(bf16[32,32,128]{2,1,0:T(8,128)(2,1)} %scan_chunks.1), calls=%async_computation.1 | async-start | bytes 524288 | tf_op jit(solution)/shard_map/all_to_all | solution.py:351
  84.7 12.4 %copy-start.1 = (f32[128,2048]{1,0:T(8,128)S(1)}, f32[128,2048]{1,0:T(8,128)}, u32[]{:S(2)}) copy-start(f32[128,2048]{1,0:T(8,128)} %adjust.2.after_ref.r_ref) | copy-start | bytes 3145732
  84.7 12.3 %copy-start.4 = (f32[2048]{0:T(1024)S(1)}, f32[2048]{0:T(1024)}, u32[]{:S(2)}) copy-start(f32[2048]{0:T(1024)} %param.18) | copy-start | bytes 24580
  97.1 1.2 %copy-start.2 = (f32[128,2048]{1,0:T(8,128)S(1)}, f32[128,2048]{1,0:T(8,128)}, u32[]{:S(2)}) copy-start(f32[128,2048]{1,0:T(8,128)} %adjust.3.o_ref) | copy-start | bytes 3145732
  98.3 3.4 %copy-start.3 = (bf16[32768,128]{1,0:T(8,128)(2,1)S(1)}, bf16[32768,128]{1,0:T(8,128)(2,1)}, u32[]{:S(2)}) copy-start(bf16[32768,128]{1,0:T(8,128)(2,1)} %all-gather.3.cloned.1.call-done) | copy-start | bytes 25165828
Sparse Core Ops, SparseCore 0:
  9.4 61.3 all-gather.2

commit v2 on v1

v2 whole, which is shorter than its diff:
```python
import jax
import jax.numpy as jnp
from jax import lax
from jax.experimental import pallas as pl
from jax.experimental.pallas import tpu as pltpu
from jax.sharding import Mesh
from jax.sharding import PartitionSpec as P

HEAD = 64
PAIR = 2 * HEAD
SMALL = 16
DP = ("dp_0", "dp_1")
GROUP = 4
FLOPS_PER_US = 500_000_000
F32 = jnp.float32
BF16 = jnp.bfloat16


def dot(left, right):
    return lax.dot_general(left, right, (((1,), (0,)), ((), ())), preferred_element_type=F32)


def dot_nt(left, right):
    return lax.dot_general(left, right, (((1,), (1,)), ((), ())), preferred_element_type=F32)


def split(value):
    high = value.astype(BF16)
    low = (value - high.astype(F32)).astype(BF16)
    return high, low


def lanes(*parts):
    return jnp.concatenate(parts, axis=1)


def rows(*parts):
    return jnp.concatenate(parts, axis=0)


def half_turn(value):
    return pltpu.roll(value, HEAD, 1)


def product(left, right):
    count = left[0].shape[0]
    both = dot(rows(*left), lanes(*right))
    return both[:count, :PAIR] + (both[:count, PAIR:] + both[count:, :PAIR])


def iota(shape, dim):
    return lax.broadcasted_iota(jnp.int32, shape, dim)


def same_head():
    return (iota((PAIR, PAIR), 0) // HEAD == iota((PAIR, PAIR), 1) // HEAD).astype(F32).astype(BF16)


def spread_kernel_table(table_ref, length):
    row = iota((length, length), 0)
    col = iota((length, length), 1)
    for s in range(SMALL):
        table_ref[:, s * length : (s + 1) * length] = (
            (row == (col // SMALL) * SMALL + s).astype(F32).astype(BF16)
        )


def inverses(matrices, table_ref, length):
    blocks = length // SMALL
    lane_block = iota((SMALL, length), 1) // SMALL
    packed = []
    for m in matrices:
        compact = jnp.zeros((SMALL, length), F32)
        for at in range(blocks):
            compact = jnp.where(lane_block == at, m[at * SMALL : (at + 1) * SMALL], compact)
        packed.append(compact)
    high, low = split(rows(*packed))
    tall = high.shape[0]
    left = rows(high, low)
    eye = (iota((SMALL, length), 1) % SMALL == iota((SMALL, length), 0)).astype(F32)
    solved = [eye for _ in matrices]
    for s in range(0, SMALL, 2):
        both = dot(left, table_ref[:, s * length : (s + 2) * length])
        both = both[:tall] + both[tall:]
        for step in range(2):
            if s + step + 1 == SMALL:
                break
            column = both[:, step * length : (step + 1) * length]
            solved = [
                x - column[i * SMALL : (i + 1) * SMALL] * x[s + step : s + step + 1] for i, x in enumerate(solved)
            ]
    own = [(lane_block == at).astype(F32).astype(BF16) for at in range(blocks)]
    parts = [tuple(rows(*(p * o for o in own)) for p in split(x)) for x in solved]
    pieces = [split(m) for m in matrices]
    apart = iota((length, length), 0) ^ iota((length, length), 1)
    block = SMALL
    while block < length:
        spans = range(0, length, 2 * block)
        odd = lambda m: rows(*(m[at + block : at + 2 * block] for at in spans))
        here = odd(((apart >= block) & (apart < 2 * block)).astype(F32).astype(BF16))
        gap = jnp.zeros((block, length), BF16)
        wide = lambda m: rows(*(x for i in range(len(spans)) for x in (gap, m[i * block : (i + 1) * block])))
        put = lambda m, t: rows(
            *(
                x
                for i, at in enumerate(spans)
                for x in (m[at : at + block], m[at + block : at + 2 * block] - t[i * block : (i + 1) * block])
            )
        )
        inner = [split(product((odd(h) * here, odd(l) * here), x)) for (h, l), x in zip(pieces, parts)]
        taken = [
            split(product((odd(h), odd(l)), (wide(dh), wide(dl)))) for (h, l), (dh, dl) in zip(parts, inner)
        ]
        parts = [(put(h, th), put(l, tl)) for (h, l), (th, tl) in zip(parts, taken)]
        block *= 2
    return parts


def paired_left(value, first):
    high, low = split(value)
    turned = half_turn(value - high.astype(F32)).astype(BF16)
    return lanes(jnp.where(first, high, turned), high), lanes(jnp.where(first, turned, high), high)


def paired_right(high, low):
    gap = jnp.zeros((HEAD, high.shape[1]), BF16)
    return (
        rows(high[:HEAD], high[:HEAD], low[:HEAD], gap),
        rows(high[HEAD:], high[HEAD:], gap, low[HEAD:]),
    )


def local_kernel(
    k_ref, v_ref, dl_ref, rl_ref, du_ref, ru_ref, base_ref, msg_ref, inner_ref, right_ref, scale_ref, centre_ref, table_ref
):
    length = k_ref.shape[0]

    @pl.when(pl.program_id(0) == 0)
    def _():
        spread_kernel_table(table_ref, length)

    row = iota((length, length), 0)
    col = iota((length, length), 1)
    strict = row > col
    lower = (row >= col).astype(F32).astype(BF16)
    lower_twice = lanes(lower, lower)
    ones = same_head()
    ones_twice = rows(ones, ones)
    squashed = jnp.tanh(dl_ref[...].astype(F32)).astype(BF16)
    decay_pre = (base_ref[...] + dot(squashed, du_ref[...])).astype(BF16).astype(F32)
    rate_pre = dot(rl_ref[...], ru_ref[...]).astype(BF16).astype(F32)
    decays = (-0.6065306597126334) / (1.0 + jnp.exp(-decay_pre))
    rates = 0.5 + 0.5 * jnp.tanh(0.5 * rate_pre)
    first = iota((length, PAIR), 1) < HEAD
    second_half = iota((HEAD, PAIR), 1) >= HEAD
    diagonal = iota((HEAD, PAIR), 0) == iota((HEAD, PAIR), 1)
    pairs = k_ref.shape[1] // PAIR
    stage = []
    lower_parts = []
    for p in range(pairs):
        span = slice(p * PAIR, (p + 1) * PAIR)
        k = k_ref[:, span].astype(F32)
        v = v_ref[:, span]
        v_turned = half_turn(v.astype(F32)).astype(BF16)
        log_decay = decays[:, span]
        squares = dot(lanes(*split(k * k)), ones_twice)
        unit = k * lax.rsqrt(1.0 + squares)
        erase = unit * rates[:, span]
        running = dot(lower_twice, rows(*split(log_decay)))
        before = running - log_decay
        centre = running[length // 2 : length // 2 + 1]
        final = running[length - 1 :]
        back = jnp.exp(centre - running)
        centre_decay = jnp.exp(centre)
        scale_ref[:, span] = jnp.exp(running - centre)
        centre_ref[:, span] = centre_decay
        columns = rows(jnp.exp(final - centre), jnp.exp(final) - 1.0, jnp.zeros((6, PAIR), F32)).T
        rest_decay = columns[:, :1]
        keep = columns[:, 1:2]
        erase_from = unit * jnp.exp(before - centre)
        key_to = (k * back).T
        erase_to = (erase * back).T
        right = split(lanes(key_to, erase_to))
        right_ref[p, 0], right_ref[p, 1] = right
        key_end = split(key_to * rest_decay)
        erase_end = split(erase_to * rest_decay)
        erase_start = erase_from * centre_decay
        starts = (erase_start, half_turn(erase_start))
        for h, (left, side) in enumerate(zip(paired_left(erase_from, first), paired_right(*right))):
            pairings = dot(left, side)
            key_pairs = split(jnp.where(strict, pairings[:, :length], 0.0))
            lower_parts.append(jnp.where(strict, pairings[:, length:], 0.0))
            half = slice(h * HEAD, (h + 1) * HEAD)
            value = v if h else v_turned
            applied = dot(
                rows(lanes(*key_pairs), lanes(key_end[0][half], key_end[1][half])), rows(value, value)
            )
            stage.append(
                dict(
                    sides=split(jnp.where(first, starts[h], applied[:length])),
                    gained=applied[length:],
                    erase_end=(erase_end[0][half], erase_end[1][half]),
                    keep=keep[half],
                )
            )
    solved = inverses(lower_parts, table_ref, length)
    for i, (s, m) in enumerate(zip(stage, solved)):
        inner = split(product(m, s["sides"]))
        inner_ref[i, 0], inner_ref[i, 1] = inner
        ended = product(s["erase_end"], inner)
        gained = jnp.where(second_half, s["gained"], jnp.where(diagonal, s["keep"], 0.0))
        msg_ref[i] = (gained - ended).astype(BF16)


def read_kernel(q_ref, v_ref, scale_ref, centre_ref, right_ref, inner_ref, out_ref, token_ref):
    length = q_ref.shape[0]
    token_ref[...] = jnp.zeros_like(token_ref)
    within = iota((length, length), 0) >= iota((length, length), 1)
    first = iota((length, PAIR), 1) < HEAD
    for p in range(q_ref.shape[1] // PAIR):
        span = slice(p * PAIR, (p + 1) * PAIR)
        v = v_ref[:, span]
        v_turned = half_turn(v.astype(F32)).astype(BF16)
        read_mid = q_ref[:, span].astype(F32) * scale_ref[:, span]
        read_start = read_mid * centre_ref[:, span]
        starts = (read_start, half_turn(read_start))
        sides = paired_right(right_ref[p, 0], right_ref[p, 1])
        for h, (left, side) in enumerate(zip(paired_left(read_mid, first), sides)):
            pairings = dot(left, side)
            read_keys = split(jnp.where(within, pairings[:, :length], 0.0))
            read_erase = split(jnp.where(within, pairings[:, length:], 0.0))
            value = v if h else v_turned
            applied = dot(lanes(*read_keys), rows(value, value))
            taken = product(read_erase, (inner_ref[2 * p + h, 0], inner_ref[2 * p + h, 1]))
            high, low = split(jnp.where(first, starts[h], applied) - taken)
            out_ref[2 * p + h, 0] = high
            out_ref[2 * p + h, 1] = low


def scan_kernel(msg_ref, after_ref, start_ref):
    first = iota((HEAD, PAIR), 1) < HEAD
    eye = (iota((HEAD, PAIR), 0) + HEAD == iota((HEAD, PAIR), 1)).astype(F32).astype(BF16)
    nothing = jnp.zeros((HEAD, PAIR), BF16)
    state = jnp.zeros((HEAD, PAIR), F32)
    chunks = msg_ref.shape[0]
    half = HEAD // 2
    for i in range(chunks):
        start_ref[i] = jnp.where(first[:half], state[:half], state[half:]).astype(BF16)
        if i + 1 < chunks:
            high, low = split(state)
            left = lanes(jnp.where(first, high, eye), jnp.where(first, low, nothing))
            here = msg_ref[i]
            here = rows(here, here)
            state = state + dot_nt(left, lanes(here, here))


def finish_kernel(start_ref, read_ref, gain_ref, w_ref, out_ref, mix_ref, here_ref, done_ref):
    copies = [pltpu.make_async_copy(w_ref.at[k], here_ref.at[k], done_ref.at[k]) for k in range(w_ref.shape[0])]
    for copy in copies:
        copy.start()
    length, width = mix_ref.shape
    ones = same_head()
    ones_twice = rows(ones, ones)
    half = HEAD // 2
    first = iota((half, PAIR), 1) < HEAD
    row = iota((HEAD, PAIR), 0)
    col = iota((HEAD, PAIR), 1)
    eyes = [(row + h * HEAD == col).astype(F32) for h in range(2)]
    for p in range(width // PAIR):
        span = slice(p * PAIR, (p + 1) * PAIR)
        one = start_ref[2 * p].astype(F32)
        two = start_ref[2 * p + 1].astype(F32)
        states = rows(
            jnp.where(first, one, 0.0),
            jnp.where(first, half_turn(one), 0.0),
            jnp.where(first, 0.0, half_turn(two)),
            jnp.where(first, 0.0, two),
        ).T
        right = rows(states[:HEAD], eyes[0], states[HEAD:], eyes[1]).astype(BF16)
        left = rows(*(lanes(read_ref[2 * p, part], read_ref[2 * p + 1, part]) for part in range(2)))
        readout = dot(left, right)
        readout = readout[:length] + readout[length:]
        average = dot(lanes(*split(readout)), ones_twice) * (1.0 / HEAD)
        centred = readout - average
        variance = dot(lanes(*split(centred * centred)), ones_twice) * (1.0 / HEAD)
        normed = centred * lax.rsqrt(variance + 1.0)
        mix_ref[:, span] = (normed * gain_ref[:, span]).astype(BF16)

    mix = mix_ref[...]
    for k in range(0, w_ref.shape[0], 2):
        copies[k].wait()
        copies[k + 1].wait()
        out_ref[:, k * 128 : (k + 2) * 128] = dot(mix, lanes(here_ref[k], here_ref[k + 1])).astype(BF16)


def budget(mib, us):
    return dict(
        compiler_params=pltpu.CompilerParams(vmem_limit_bytes=mib << 20),
        cost_estimate=pl.CostEstimate(flops=int(us * FLOPS_PER_US), transcendentals=0, bytes_accessed=1 << 20),
    )


def local_chunk(k, v, dl, rl, du, ru, base):
    length, width = k.shape
    heads = width // HEAD
    step = GROUP * HEAD
    wide = pl.BlockSpec((length, step), lambda i: (0, i))
    low = pl.BlockSpec(dl.shape, lambda i: (0, 0))
    up = pl.BlockSpec((du.shape[0], step), lambda i: (0, i))
    line = pl.BlockSpec((1, step), lambda i: (0, i))
    return pl.pallas_call(
        local_kernel,
        grid=(width // step,),
        in_specs=[wide, wide, low, low, up, up, line],
        out_specs=[
            pl.BlockSpec((GROUP, HEAD, PAIR), lambda i: (i, 0, 0)),
            pl.BlockSpec((GROUP, 2, length, PAIR), lambda i: (i, 0, 0, 0)),
            pl.BlockSpec((GROUP // 2, 2, PAIR, 2 * length), lambda i: (i, 0, 0, 0)),
            wide,
            line,
        ],
        out_shape=[
            jax.ShapeDtypeStruct((heads, HEAD, PAIR), BF16),
            jax.ShapeDtypeStruct((heads, 2, length, PAIR), BF16),
            jax.ShapeDtypeStruct((heads // 2, 2, PAIR, 2 * length), BF16),
            jax.ShapeDtypeStruct((length, width), F32),
            jax.ShapeDtypeStruct((1, width), F32),
        ],
        scratch_shapes=[pltpu.VMEM((length, SMALL * length), BF16)],
        name="local_chunk",
        **budget(60, 25),
    )(k, v, dl, rl, du, ru, base.reshape(1, width))


def chunk_reads(q, v, scale, centre, right, inner):
    length, width = q.shape
    heads = width // HEAD
    count = 2 * GROUP
    step = count * HEAD
    wide = pl.BlockSpec((length, step), lambda i: (0, i))
    per_head = pl.BlockSpec((count, 2, length, PAIR), lambda i: (i, 0, 0, 0))
    return pl.pallas_call(
        read_kernel,
        grid=(width // step,),
        in_specs=[
            wide,
            wide,
            wide,
            pl.BlockSpec((1, step), lambda i: (0, i)),
            pl.BlockSpec((count // 2, 2, PAIR, 2 * length), lambda i: (i, 0, 0, 0)),
            per_head,
        ],
        out_specs=[per_head, pl.BlockSpec((8, PAIR), lambda i: (0, 0))],
        out_shape=[
            jax.ShapeDtypeStruct((heads, 2, length, PAIR), BF16),
            jax.ShapeDtypeStruct((8, PAIR), F32),
        ],
        name="chunk_reads",
        **budget(60, 8),
    )(q, v, scale, centre, right, inner)


def scan_chunks(msg, after):
    chunks = msg.shape[0]
    return pl.pallas_call(
        scan_kernel,
        in_specs=[pl.BlockSpec(memory_space=pltpu.VMEM), pl.BlockSpec(memory_space=pltpu.HBM)],
        out_shape=jax.ShapeDtypeStruct((chunks, HEAD // 2, PAIR), BF16),
        name="scan_chunks",
        **budget(4, 6),
    )(msg, after)


def finish(starts, reads, gain, weight):
    length = reads.shape[2]
    width = gain.shape[0]
    return pl.pallas_call(
        finish_kernel,
        in_specs=[pl.BlockSpec(memory_space=pltpu.VMEM)] * 3 + [pl.BlockSpec(memory_space=pltpu.HBM)],
        out_shape=jax.ShapeDtypeStruct((length, weight.shape[0] * weight.shape[2]), BF16),
        scratch_shapes=[
            pltpu.VMEM((length, width), BF16),
            pltpu.VMEM(weight.shape, BF16),
            pltpu.SemaphoreType.DMA((weight.shape[0],)),
        ],
        name="finish",
        **budget(60, 12),
    )(starts, reads, gain.reshape(1, width), weight)


def per_device(
    query_rows, key_rows, value_rows, decay_low, rate_low, decay_up, rate_up, decay_base, norm_gain, out_weight
):
    columns = lax.all_gather(out_weight, DP)
    msg, inner, right, scale, centre = local_chunk(
        key_rows[0], value_rows[0], decay_low[0], rate_low[0], decay_up, rate_up, decay_base
    )
    here = lax.all_to_all(msg, "sp", split_axis=0, concat_axis=0, tiled=True)
    reads, token = chunk_reads(query_rows[0], value_rows[0], scale, centre, right, inner)
    starts = scan_chunks(here, token)
    back = lax.all_to_all(starts, "sp", split_axis=0, concat_axis=0, tiled=True)
    return finish(back, reads, norm_gain, columns)[None]


def solution(mesh):
    split_mesh = Mesh(mesh.devices.reshape(mesh.shape["sp"], 8, 2), ("sp", "dp_0", "dp_1"))
    placed = (
        P(DP, "sp", None),
        P(DP, "sp", None),
        P(DP, "sp", None),
        P(DP, "sp", None),
        P(DP, "sp", None),
        P(),
        P(),
        P(),
        P(),
        P(None, DP),
    )
    return jax.shard_map(
        per_device, mesh=split_mesh, in_specs=placed, out_specs=P(DP, "sp", None), check_vma=False
    )
```

time: 117 us -> 105 us (0.90)
  blocking collectives: 0 us -> 16.9 us
  waiting for transfers between devices: 21.6 us -> 10 us
  Pallas kernels: 57.7 us -> 50.5 us
  local copies, waits for them, and re-layouts: 5.84 us -> 0.67 us
  starting transfers between devices: 17.8 us -> 13.2 us
    all_to_all x0 -> x1, blocking collectives: none -> 16.9 us  [per_device(): back = lax.all_to_all(starts, 'sp', split_axis=0, concat_axis=0, tiled=True)]
    all_to_all x1 -> x0, waiting for transfers between devices: 7.69 us -> none  [per_device(): back = lax.all_to_all(starts, 'sp', split_axis=0, concat_axis=0, tiled=True)]
    pallas_call x1, Pallas kernels: 36.2 us -> 29.2 us  [local_chunk(): pl.pallas_call(local_kernel, grid=(width // step,), in_specs=[wide, wide,...]
    unnamed x10 -> x2, local copies, waits for them, and re-layouts: 5.84 us -> 0.67 us
    all_to_all x1 -> x0, starting transfers between devices: 4.67 us -> none  [per_device(): back = lax.all_to_all(starts, 'sp', split_axis=0, concat_axis=0, tiled=True)]
    all_to_all x1, waiting for transfers between devices: 13.2 us -> 9.29 us  [per_device(): here = lax.all_to_all(msg, 'sp', split_axis=0, concat_axis=0, tiled=True)]
    pallas_call x2 -> x1, Pallas kernels: 9.18 us -> 8.47 us  [chunk_reads(): pl.pallas_call(read_kernel, grid=(width // step,), in_specs=[wide, wide,...]
  transfers between devices with their start and end apart: 3 -> 2, of which waited for: 2 -> 1; matrix products, arithmetic and copies ran while one was open for 0% -> 0% of each run, Pallas kernels for 43% -> 40%
where the time goes in v2:
time: 105 us
  Pallas kernels  50.5 us (48%)
  blocking collectives  16.9 us (16%)
  between operations  13.4 us (13%)
  starting transfers between devices  13.2 us (13%)
  waiting for transfers between devices  10 us (10%)
    pallas_call x1, Pallas kernels, local_chunk(): pl.pallas_call(local_kernel, grid=(width // step,), in_specs=[wide, wide,...  29.2 us
    all_to_all x1, blocking collectives, per_device(): back = lax.all_to_all(starts, 'sp', split_axis=0, concat_axis=0, tiled=True)  16.9 us
    all_to_all x1, starting transfers between devices, per_device(): here = lax.all_to_all(msg, 'sp', split_axis=0, concat_axis=0, tiled=True)  13.2 us
    all_to_all x1, waiting for transfers between devices, per_device(): here = lax.all_to_all(msg, 'sp', split_axis=0, concat_axis=0, tiled=True)  9.29 us
    pallas_call x1, Pallas kernels, finish(): pl.pallas_call(finish_kernel, in_specs=[pl.BlockSpec(memory_space=pltpu.V...  9 us
    pallas_call x1, Pallas kernels, chunk_reads(): pl.pallas_call(read_kernel, grid=(width // step,), in_specs=[wide, wide,...  8.47 us
    pallas_call x1, Pallas kernels, scan_chunks(): pl.pallas_call(scan_kernel, in_specs=[pl.BlockSpec(memory_space=pltpu.VME...  3.76 us
  transfers between devices with their start and end apart: 2, of which 1 were waited for; matrix products, arithmetic and copies ran while one was open for 0% of the time, Pallas kernels for 40%

profile of v2, /device:TPU:8, one launch (start us, length us, event | category | flops | bytes accessed | tf_op | source)
XLA Modules:
  0.0 104.6 jit_solution(6789564881027365874)
XLA Ops:
  6.5 0.0 all-gather.3.cloned.1.call-start
  6.5 0.7 all-gather.3.cloned.1.call-update
  7.3 29.2 %local_chunk.1 = (bf16[32,64,128]{2,1,0:T(8,128)(2,1)}, bf16[32,2,128,128]{3,2,1,0:T(8,128)(2,1)}, bf16[16,2,128,256]{3,2,1,0:T(8,128)(2,1)}, f32[128,2048]{1,0:T(8,128)}, f32[1,2048]{1,0:T(1,128)}) custom-call(bf16[128,2048]{1,0:T(8,128)(2,1)} %bitcast.10, bf16[128,2048]{1,0:T(8,128)(2,1)} %bitcast.11, bf16[128,128]{1,0:T(8,128)(2,1)} %bitcast.14, ...), custom_call_target="tpu_custom_call" | custom-call | flops 12499999744 | bytes 1048576 | tf_op jit(solution)/shard_map/local_chunk/pallas_call | solution.py:311
  36.5 13.2 %all-to-all-start = ((bf16[32,64,128]{2,1,0:T(8,128)(2,1)}), bf16[32,64,128]{2,1,0:T(8,128)(2,1)S(1)}, u32[]{:S(2)}, u32[]{:S(2)}) async-start(bf16[32,64,128]{2,1,0:T(8,128)(2,1)} %get-tuple-element.12), calls=%async_computation | async-start | bytes 1048576 | tf_op jit(solution)/shard_map/all_to_all | solution.py:398
  49.7 8.5 %chunk_reads.1 = (bf16[32,2,128,128]{3,2,1,0:T(8,128)(2,1)}, f32[8,128]{1,0:T(8,128)}) custom-call(bf16[128,2048]{1,0:T(8,128)(2,1)} %bitcast.13, bf16[128,2048]{1,0:T(8,128)(2,1)} %bitcast.12, f32[128,2048]{1,0:T(8,128)} %get-tuple-element.13.scale_ref, f32[1,2048]{1,0:T(1,128)} %get-tuple-element.14.centre_ref, ...), custom_call_target="tpu_custom_call" | custom-call | flops 4000000000 | bytes 1048576 | tf_op jit(solution)/shard_map/chunk_reads/pallas_call | solution.py:342
  58.1 9.3 %all-to-all-done.msg_ref = bf16[32,64,128]{2,1,0:T(8,128)(2,1)S(1)} async-done(((bf16[32,64,128]{2,1,0:T(8,128)(2,1)}), bf16[32,64,128]{2,1,0:T(8,128)(2,1)S(1)}, u32[]{:S(2)}, u32[]{:S(2)}) %all-to-all-start) | async-done | bytes 524320 | tf_op jit(solution)/shard_map/all_to_all | solution.py:398
  67.4 0.0 copy-start
  67.4 0.7 copy-done
  68.1 3.8 %scan_chunks.1 = bf16[32,32,128]{2,1,0:T(8,128)(2,1)S(1)} custom-call(bf16[32,64,128]{2,1,0:T(8,128)(2,1)S(1)} %all-to-all-done.msg_ref, f32[8,128]{1,0:T(8,128)S(1)} %copy-done), custom_call_target="tpu_custom_call" | custom-call | flops 3000000000 | bytes 1048576 | tf_op jit(solution)/shard_map/scan_chunks/pallas_call | solution.py:365
  71.9 16.9 %all_to_all.10.start_ref = bf16[32,32,128]{2,1,0:T(8,128)(2,1)} all-to-all(bf16[32,32,128]{2,1,0:T(8,128)(2,1)S(1)} %scan_chunks.1), channel_id=1, replica_groups=mesh['sp'=32,'dp_0'=8,'dp_1'=2] {'sp'}, dimensions={0} | all-to-all | bytes 524288 | tf_op jit(solution)/shard_map/all_to_all | solution.py:401
  88.8 0.0 all-gather.3.cloned.1.call-done
  88.8 9.0 %finish.1 = bf16[128,2048]{1,0:T(8,128)(2,1)} custom-call(bf16[32,32,128]{2,1,0:T(8,128)(2,1)} %all_to_all.10.start_ref, bf16[32,2,128,128]{3,2,1,0:T(8,128)(2,1)} %get-tuple-element.18.read_ref, f32[1,2048]{1,0:T(1,128)} %bitcast.17, bf16[16,2048,128]{2,1,0:T(8,128)(2,1)} %bitcast.9), custom_call_target="tpu_custom_call" | custom-call | flops 6000000000 | bytes 1048576 | tf_op jit(solution)/shard_map/finish/pallas_call | solution.py:377
Async XLA Ops:
  6.5 82.2 %all-gather.3.cloned.1.call-start = ((), (), s32[]{:S(2)}) async-start(), calls=%async_computation.2 | async-start | bytes 8912896 | tf_op jit(solution)/shard_map/all_gather | solution.py:394
  36.5 30.9 %all-to-all-start = ((bf16[32,64,128]{2,1,0:T(8,128)(2,1)}), bf16[32,64,128]{2,1,0:T(8,128)(2,1)S(1)}, u32[]{:S(2)}, u32[]{:S(2)}) async-start(bf16[32,64,128]{2,1,0:T(8,128)(2,1)} %get-tuple-element.12), calls=%async_computation | async-start | bytes 1048576 | tf_op jit(solution)/shard_map/all_to_all | solution.py:398
  67.4 0.7 copy-start
Sparse Core Ops, SparseCore 0:
  9.4 61.4 all-gather.2

commit v3 on v2

--- a/solution.py
+++ b/solution.py
@@ -10,7 +10,10 @@
 PAIR = 2 * HEAD
 SMALL = 16
 DP = ("dp_0", "dp_1")
-GROUP = 4
+GROUP = 16
+TOGETHER = 8
+ABREAST = 8
+BLOCKS = 8
 FLOPS_PER_US = 500_000_000
 F32 = jnp.float32
 BF16 = jnp.bfloat16
@@ -89,6 +92,8 @@
             solved = [
                 x - column[i * SMALL : (i + 1) * SMALL] * x[s + step : s + step + 1] for i, x in enumerate(solved)
             ]
+        if s % 4:
+            yield None
     own = [(lane_block == at).astype(F32).astype(BF16) for at in range(blocks)]
     parts = [tuple(rows(*(p * o for o in own)) for p in split(x)) for x in solved]
     pieces = [split(m) for m in matrices]
@@ -107,13 +112,15 @@
                 for x in (m[at : at + block], m[at + block : at + 2 * block] - t[i * block : (i + 1) * block])
             )
         )
+        yield None
         inner = [split(product((odd(h) * here, odd(l) * here), x)) for (h, l), x in zip(pieces, parts)]
+        yield None
         taken = [
             split(product((odd(h), odd(l)), (wide(dh), wide(dl)))) for (h, l), (dh, dl) in zip(parts, inner)
         ]
         parts = [(put(h, th), put(l, tl)) for (h, l), (th, tl) in zip(parts, taken)]
         block *= 2
-    return parts
+    yield parts
 
 
 def paired_left(value, first):
@@ -147,26 +154,25 @@
     ones = same_head()
     ones_twice = rows(ones, ones)
     squashed = jnp.tanh(dl_ref[...].astype(F32)).astype(BF16)
-    decay_pre = (base_ref[...] + dot(squashed, du_ref[...])).astype(BF16).astype(F32)
-    rate_pre = dot(rl_ref[...], ru_ref[...]).astype(BF16).astype(F32)
-    decays = (-0.6065306597126334) / (1.0 + jnp.exp(-decay_pre))
-    rates = 0.5 + 0.5 * jnp.tanh(0.5 * rate_pre)
     first = iota((length, PAIR), 1) < HEAD
     second_half = iota((HEAD, PAIR), 1) >= HEAD
     diagonal = iota((HEAD, PAIR), 0) == iota((HEAD, PAIR), 1)
-    pairs = k_ref.shape[1] // PAIR
-    stage = []
-    lower_parts = []
-    for p in range(pairs):
+
+    def prepare(p):
         span = slice(p * PAIR, (p + 1) * PAIR)
+        decay_pre = (base_ref[:, span] + dot(squashed, du_ref[:, span])).astype(BF16).astype(F32)
+        rate_pre = dot(rl_ref[...], ru_ref[:, span]).astype(BF16).astype(F32)
+        yield None
+        log_decay = (-0.6065306597126334) / (1.0 + jnp.exp(-decay_pre))
+        rate = 0.5 + 0.5 * jnp.tanh(0.5 * rate_pre)
         k = k_ref[:, span].astype(F32)
         v = v_ref[:, span]
         v_turned = half_turn(v.astype(F32)).astype(BF16)
-        log_decay = decays[:, span]
         squares = dot(lanes(*split(k * k)), ones_twice)
         unit = k * lax.rsqrt(1.0 + squares)
-        erase = unit * rates[:, span]
+        erase = unit * rate
         running = dot(lower_twice, rows(*split(log_decay)))
+        yield None
         before = running - log_decay
         centre = running[length // 2 : length // 2 + 1]
         final = running[length - 1 :]
@@ -186,35 +192,54 @@
         erase_end = split(erase_to * rest_decay)
         erase_start = erase_from * centre_decay
         starts = (erase_start, half_turn(erase_start))
-        for h, (left, side) in enumerate(zip(paired_left(erase_from, first), paired_right(*right))):
-            pairings = dot(left, side)
+        sides = zip(paired_left(erase_from, first), paired_right(*right))
+        yield None
+        paired = [dot(left, side) for left, side in sides]
+        yield None
+        made = []
+        for h, pairings in enumerate(paired):
             key_pairs = split(jnp.where(strict, pairings[:, :length], 0.0))
-            lower_parts.append(jnp.where(strict, pairings[:, length:], 0.0))
             half = slice(h * HEAD, (h + 1) * HEAD)
             value = v if h else v_turned
             applied = dot(
                 rows(lanes(*key_pairs), lanes(key_end[0][half], key_end[1][half])), rows(value, value)
             )
-            stage.append(
+            made.append(
                 dict(
+                    head=2 * p + h,
+                    lower=jnp.where(strict, pairings[:, length:], 0.0),
                     sides=split(jnp.where(first, starts[h], applied[:length])),
                     gained=applied[length:],
                     erase_end=(erase_end[0][half], erase_end[1][half]),
                     keep=keep[half],
                 )
             )
-    solved = inverses(lower_parts, table_ref, length)
-    for i, (s, m) in enumerate(zip(stage, solved)):
-        inner = split(product(m, s["sides"]))
-        inner_ref[i, 0], inner_ref[i, 1] = inner
-        ended = product(s["erase_end"], inner)
-        gained = jnp.where(second_half, s["gained"], jnp.where(diagonal, s["keep"], 0.0))
-        msg_ref[i] = (gained - ended).astype(BF16)
-
-
-def read_kernel(q_ref, v_ref, scale_ref, centre_ref, right_ref, inner_ref, out_ref, token_ref):
+        yield made
+
+    def solve(stage):
+        for solved in inverses([s["lower"] for s in stage], table_ref, length):
+            yield
+        inners = [split(product(m, s["sides"])) for s, m in zip(stage, solved)]
+        yield
+        for s, inner in zip(stage, inners):
+            head = s["head"]
+            inner_ref[head, 0], inner_ref[head, 1] = inner
+            ended = product(s["erase_end"], inner)
+            gained = jnp.where(second_half, s["gained"], jnp.where(diagonal, s["keep"], 0.0))
+            msg_ref[head] = (gained - ended).astype(BF16)
+
+    pairs = k_ref.shape[1] // PAIR
+    stage = []
+    for start in range(0, pairs, TOGETHER):
+        for made in zip(*(prepare(p) for p in range(start, min(start + TOGETHER, pairs)))):
+            pass
+        stage += [head for pair in made for head in pair]
+    for _ in solve(stage):
+        pass
+
+
+def read_kernel(q_ref, v_ref, scale_ref, centre_ref, right_ref, inner_ref, out_ref):
     length = q_ref.shape[0]
-    token_ref[...] = jnp.zeros_like(token_ref)
     within = iota((length, length), 0) >= iota((length, length), 1)
     first = iota((length, PAIR), 1) < HEAD
     for p in range(q_ref.shape[1] // PAIR):
@@ -237,7 +262,7 @@
             out_ref[2 * p + h, 1] = low
 
 
-def scan_kernel(msg_ref, after_ref, start_ref):
+def scan_kernel(msg_ref, start_ref):
     first = iota((HEAD, PAIR), 1) < HEAD
     eye = (iota((HEAD, PAIR), 0) + HEAD == iota((HEAD, PAIR), 1)).astype(F32).astype(BF16)
     nothing = jnp.zeros((HEAD, PAIR), BF16)
@@ -266,7 +291,7 @@
     row = iota((HEAD, PAIR), 0)
     col = iota((HEAD, PAIR), 1)
     eyes = [(row + h * HEAD == col).astype(F32) for h in range(2)]
-    for p in range(width // PAIR):
+    def mixed(p):
         span = slice(p * PAIR, (p + 1) * PAIR)
         one = start_ref[2 * p].astype(F32)
         two = start_ref[2 * p + 1].astype(F32)
@@ -277,20 +302,29 @@
             jnp.where(first, 0.0, two),
         ).T
         right = rows(states[:HEAD], eyes[0], states[HEAD:], eyes[1]).astype(BF16)
+        yield
         left = rows(*(lanes(read_ref[2 * p, part], read_ref[2 * p + 1, part]) for part in range(2)))
         readout = dot(left, right)
+        yield
         readout = readout[:length] + readout[length:]
         average = dot(lanes(*split(readout)), ones_twice) * (1.0 / HEAD)
+        yield
         centred = readout - average
         variance = dot(lanes(*split(centred * centred)), ones_twice) * (1.0 / HEAD)
+        yield
         normed = centred * lax.rsqrt(variance + 1.0)
         mix_ref[:, span] = (normed * gain_ref[:, span]).astype(BF16)
-
+        yield
+
+    for start in range(0, width // PAIR, ABREAST):
+        for _ in zip(*(mixed(p) for p in range(start, start + ABREAST))):
+            pass
     mix = mix_ref[...]
-    for k in range(0, w_ref.shape[0], 2):
-        copies[k].wait()
-        copies[k + 1].wait()
-        out_ref[:, k * 128 : (k + 2) * 128] = dot(mix, lanes(here_ref[k], here_ref[k + 1])).astype(BF16)
+    for k in range(0, w_ref.shape[0], BLOCKS):
+        for copy in copies[k : k + BLOCKS]:
+            copy.wait()
+        right = lanes(*(here_ref[j] for j in range(k, k + BLOCKS)))
+        out_ref[:, k * 128 : (k + BLOCKS) * 128] = dot(mix, right).astype(BF16)
 
 
 def budget(mib, us):
@@ -335,7 +369,7 @@
 def chunk_reads(q, v, scale, centre, right, inner):
     length, width = q.shape
     heads = width // HEAD
-    count = 2 * GROUP
+    count = GROUP // 2
     step = count * HEAD
     wide = pl.BlockSpec((length, step), lambda i: (0, i))
     per_head = pl.BlockSpec((count, 2, length, PAIR), lambda i: (i, 0, 0, 0))
@@ -350,25 +384,21 @@
             pl.BlockSpec((count // 2, 2, PAIR, 2 * length), lambda i: (i, 0, 0, 0)),
             per_head,
         ],
-        out_specs=[per_head, pl.BlockSpec((8, PAIR), lambda i: (0, 0))],
-        out_shape=[
-            jax.ShapeDtypeStruct((heads, 2, length, PAIR), BF16),
-            jax.ShapeDtypeStruct((8, PAIR), F32),
-        ],
+        out_specs=per_head,
+        out_shape=jax.ShapeDtypeStruct((heads, 2, length, PAIR), BF16),
         name="chunk_reads",
         **budget(60, 8),
     )(q, v, scale, centre, right, inner)
 
 
-def scan_chunks(msg, after):
+def scan_chunks(msg):
     chunks = msg.shape[0]
     return pl.pallas_call(
         scan_kernel,
-        in_specs=[pl.BlockSpec(memory_space=pltpu.VMEM), pl.BlockSpec(memory_space=pltpu.HBM)],
         out_shape=jax.ShapeDtypeStruct((chunks, HEAD // 2, PAIR), BF16),
         name="scan_chunks",
         **budget(4, 6),
-    )(msg, after)
+    )(msg)
 
 
 def finish(starts, reads, gain, weight):
@@ -396,8 +426,9 @@
         key_rows[0], value_rows[0], decay_low[0], rate_low[0], decay_up, rate_up, decay_base
     )
     here = lax.all_to_all(msg, "sp", split_axis=0, concat_axis=0, tiled=True)
-    reads, token = chunk_reads(query_rows[0], value_rows[0], scale, centre, right, inner)
-    starts = scan_chunks(here, token)
+    reads = chunk_reads(query_rows[0], value_rows[0], scale, centre, right, inner)
+    here, reads = lax.optimization_barrier((here, reads))
+    starts = scan_chunks(here)
     back = lax.all_to_all(starts, "sp", split_axis=0, concat_axis=0, tiled=True)
     return finish(back, reads, norm_gain, columns)[None]
 

time: 105 us -> 87.4 us (0.83)
  the two profiles are of different devices: /device:TPU:8 before, /device:TPU:1 now
where the time goes in v3:
time: 87.4 us; the launch traced here: 87 us
  Pallas kernels  33.1 us (38%)
  blocking collectives  15.6 us (18%)
  starting transfers between devices  13.7 us (16%)
  between operations  13.4 us (15%)
  waiting for transfers between devices  11.2 us (13%)
    all_to_all x1, blocking collectives, per_device(): back = lax.all_to_all(starts, 'sp', split_axis=0, concat_axis=0, tiled=True)  15.6 us
    pallas_call x1, Pallas kernels, local_chunk(): pl.pallas_call(local_kernel, grid=(width // step,), in_specs=[wide, wide,...  14.3 us
    all_to_all x1, starting transfers between devices, per_device(): here = lax.all_to_all(msg, 'sp', split_axis=0, concat_axis=0, tiled=True)  13.7 us
    pallas_call x1, Pallas kernels, chunk_reads(): pl.pallas_call(read_kernel, grid=(width // step,), in_specs=[wide, wide,...  8.43 us
    all_to_all x1, waiting for transfers between devices, per_device(): here = lax.all_to_all(msg, 'sp', split_axis=0, concat_axis=0, tiled=True)  7.85 us
    pallas_call x1, Pallas kernels, finish(): pl.pallas_call(finish_kernel, in_specs=[pl.BlockSpec(memory_space=pltpu.V...  6.61 us
    pallas_call x1, Pallas kernels, scan_chunks(): pl.pallas_call(scan_kernel, out_shape=jax.ShapeDtypeStruct((chunks, HEAD...  3.76 us
    all_gather x1, waiting for transfers between devices, per_device(): columns = lax.all_gather(out_weight, DP)  2.61 us
  transfers between devices with their start and end apart: 2, of which 2 were waited for; matrix products, arithmetic and copies ran while one was open for 0% of the time, Pallas kernels for 30%

profile of v3, /device:TPU:1, one launch (start us, length us, event | category | flops | bytes accessed | tf_op | source)
XLA Modules:
  0.0 87.0 jit_solution(5451666891964437864)
XLA Ops:
  6.5 0.0 all-gather.3.cloned.1.call-start
  6.5 0.7 all-gather.3.cloned.1.call-update
  7.3 14.3 %local_chunk.1 = (bf16[32,64,128]{2,1,0:T(8,128)(2,1)}, bf16[32,2,128,128]{3,2,1,0:T(8,128)(2,1)}, bf16[16,2,128,256]{3,2,1,0:T(8,128)(2,1)}, f32[128,2048]{1,0:T(8,128)}, f32[1,2048]{1,0:T(1,128)}) custom-call(bf16[128,2048]{1,0:T(8,128)(2,1)} %bitcast.10, bf16[128,2048]{1,0:T(8,128)(2,1)} %bitcast.11, bf16[128,128]{1,0:T(8,128)(2,1)} %bitcast.14, ...), custom_call_target="tpu_custom_call" | custom-call | flops 12499999744 | bytes 1048576 | tf_op jit(solution)/shard_map/local_chunk/pallas_call | solution.py:345
  21.6 13.7 %all-to-all-start = ((bf16[32,64,128]{2,1,0:T(8,128)(2,1)}), bf16[32,64,128]{2,1,0:T(8,128)(2,1)S(1)}, u32[]{:S(2)}, u32[]{:S(2)}) async-start(bf16[32,64,128]{2,1,0:T(8,128)(2,1)} %get-tuple-element.12), calls=%async_computation | async-start | bytes 1048576 | tf_op jit(solution)/shard_map/all_to_all | solution.py:428
  35.3 8.4 %chunk_reads.1.read_ref = bf16[32,2,128,128]{3,2,1,0:T(8,128)(2,1)} custom-call(bf16[128,2048]{1,0:T(8,128)(2,1)} %bitcast.13, bf16[128,2048]{1,0:T(8,128)(2,1)} %bitcast.12, f32[128,2048]{1,0:T(8,128)} %get-tuple-element.13.scale_ref, f32[1,2048]{1,0:T(1,128)} %get-tuple-element.14.centre_ref, bf16[16,2,128,256]{3,2,1,0:T(8,128)(2,1)} %get-tuple-element.15.right_ref, ...), custom_call_target="tpu_custom_call" | custom-call | flops 4000000000 | bytes 1048576 | tf_op jit(solution)/shard_map/chunk_reads/pallas_call | solution.py:376
  43.8 7.9 %all-to-all-done.msg_ref = bf16[32,64,128]{2,1,0:T(8,128)(2,1)S(1)} async-done(((bf16[32,64,128]{2,1,0:T(8,128)(2,1)}), bf16[32,64,128]{2,1,0:T(8,128)(2,1)S(1)}, u32[]{:S(2)}, u32[]{:S(2)}) %all-to-all-start) | async-done | bytes 524320 | tf_op jit(solution)/shard_map/all_to_all | solution.py:428
  51.6 3.8 %scan_chunks.1 = bf16[32,32,128]{2,1,0:T(8,128)(2,1)S(1)} custom-call(bf16[32,64,128]{2,1,0:T(8,128)(2,1)S(1)} %all-to-all-done.msg_ref), custom_call_target="tpu_custom_call" | custom-call | flops 3000000000 | bytes 1048576 | tf_op jit(solution)/shard_map/scan_chunks/pallas_call | solution.py:396
  55.4 15.6 %all_to_all.10.start_ref = bf16[32,32,128]{2,1,0:T(8,128)(2,1)} all-to-all(bf16[32,32,128]{2,1,0:T(8,128)(2,1)S(1)} %scan_chunks.1), channel_id=1, replica_groups=mesh['sp'=32,'dp_0'=8,'dp_1'=2] {'sp'}, dimensions={0} | all-to-all | bytes 524288 | tf_op jit(solution)/shard_map/all_to_all | solution.py:432
  70.9 2.6 %all-gather.3.cloned.1.call-done = bf16[32768,128]{1,0:T(8,128)(2,1)} async-done(((bf16[2048,128]{1,0:T(8,128)(2,1)}), bf16[32768,128]{1,0:T(8,128)(2,1)}) %all-gather.3.cloned.1.call-update) | async-done | bytes 8388624 | tf_op jit(solution)/shard_map/all_gather | solution.py:424
  73.5 6.6 %finish.1 = bf16[128,2048]{1,0:T(8,128)(2,1)} custom-call(bf16[32,32,128]{2,1,0:T(8,128)(2,1)} %all_to_all.10.start_ref, bf16[32,2,128,128]{3,2,1,0:T(8,128)(2,1)} %chunk_reads.1.read_ref, f32[1,2048]{1,0:T(1,128)} %bitcast.17, bf16[16,2048,128]{2,1,0:T(8,128)(2,1)} %bitcast.9), custom_call_target="tpu_custom_call" | custom-call | flops 6000000000 | bytes 1048576 | tf_op jit(solution)/shard_map/finish/pallas_call | solution.py:407
Async XLA Ops:
  6.5 67.0 %all-gather.3.cloned.1.call-start = ((), (), s32[]{:S(2)}) async-start(), calls=%async_computation.2 | async-start | bytes 8912896 | tf_op jit(solution)/shard_map/all_gather | solution.py:424
  21.6 30.0 %all-to-all-start = ((bf16[32,64,128]{2,1,0:T(8,128)(2,1)}), bf16[32,64,128]{2,1,0:T(8,128)(2,1)S(1)}, u32[]{:S(2)}, u32[]{:S(2)}) async-start(bf16[32,64,128]{2,1,0:T(8,128)(2,1)} %get-tuple-element.12), calls=%async_computation | async-start | bytes 1048576 | tf_op jit(solution)/shard_map/all_to_all | solution.py:428
Sparse Core Ops, SparseCore 0:
  9.4 64.0 all-gather.2

commit v4 on v3

--- a/solution.py
+++ b/solution.py
@@ -13,7 +13,8 @@
 GROUP = 16
 TOGETHER = 8
 ABREAST = 8
-BLOCKS = 8
+READS = 4
+BLOCKS = 4
 FLOPS_PER_US = 500_000_000
 F32 = jnp.float32
 BF16 = jnp.bfloat16
@@ -242,7 +243,8 @@
     length = q_ref.shape[0]
     within = iota((length, length), 0) >= iota((length, length), 1)
     first = iota((length, PAIR), 1) < HEAD
-    for p in range(q_ref.shape[1] // PAIR):
+
+    def read(p):
         span = slice(p * PAIR, (p + 1) * PAIR)
         v = v_ref[:, span]
         v_turned = half_turn(v.astype(F32)).astype(BF16)
@@ -250,16 +252,27 @@
         read_start = read_mid * centre_ref[:, span]
         starts = (read_start, half_turn(read_start))
         sides = paired_right(right_ref[p, 0], right_ref[p, 1])
-        for h, (left, side) in enumerate(zip(paired_left(read_mid, first), sides)):
-            pairings = dot(left, side)
+        paired = [dot(left, side) for left, side in zip(paired_left(read_mid, first), sides)]
+        yield
+        parts = []
+        for h, pairings in enumerate(paired):
             read_keys = split(jnp.where(within, pairings[:, :length], 0.0))
             read_erase = split(jnp.where(within, pairings[:, length:], 0.0))
             value = v if h else v_turned
             applied = dot(lanes(*read_keys), rows(value, value))
             taken = product(read_erase, (inner_ref[2 * p + h, 0], inner_ref[2 * p + h, 1]))
+            parts.append((applied, taken))
+        yield
+        for h, (applied, taken) in enumerate(parts):
             high, low = split(jnp.where(first, starts[h], applied) - taken)
             out_ref[2 * p + h, 0] = high
             out_ref[2 * p + h, 1] = low
+        yield
+
+    pairs = q_ref.shape[1] // PAIR
+    for start in range(0, pairs, READS):
+        for _ in zip(*(read(p) for p in range(start, min(start + READS, pairs)))):
+            pass
 
 
 def scan_kernel(msg_ref, start_ref):
@@ -279,7 +292,7 @@
             state = state + dot_nt(left, lanes(here, here))
 
 
-def finish_kernel(start_ref, read_ref, gain_ref, w_ref, out_ref, mix_ref, here_ref, done_ref):
+def finish_kernel(start_ref, early_ref, late_ref, gain_ref, w_ref, out_ref, mix_ref, here_ref, done_ref):
     copies = [pltpu.make_async_copy(w_ref.at[k], here_ref.at[k], done_ref.at[k]) for k in range(w_ref.shape[0])]
     for copy in copies:
         copy.start()
@@ -303,7 +316,9 @@
         ).T
         right = rows(states[:HEAD], eyes[0], states[HEAD:], eyes[1]).astype(BF16)
         yield
-        left = rows(*(lanes(read_ref[2 * p, part], read_ref[2 * p + 1, part]) for part in range(2)))
+        early = early_ref.shape[0] // 2
+        read_ref, q = (early_ref, p) if p < early else (late_ref, p - early)
+        left = rows(*(lanes(read_ref[2 * q, part], read_ref[2 * q + 1, part]) for part in range(2)))
         readout = dot(left, right)
         yield
         readout = readout[:length] + readout[length:]
@@ -366,28 +381,30 @@
     )(k, v, dl, rl, du, ru, base.reshape(1, width))
 
 
-def chunk_reads(q, v, scale, centre, right, inner):
+def chunk_reads(part, parts, q, v, scale, centre, right, inner):
     length, width = q.shape
-    heads = width // HEAD
+    heads = width // HEAD // parts
     count = GROUP // 2
     step = count * HEAD
-    wide = pl.BlockSpec((length, step), lambda i: (0, i))
-    per_head = pl.BlockSpec((count, 2, length, PAIR), lambda i: (i, 0, 0, 0))
+    steps = heads // count
+    at = lambda i: part * steps + i
+    wide = pl.BlockSpec((length, step), lambda i: (0, at(i)))
+    per_head = lambda place: pl.BlockSpec((count, 2, length, PAIR), lambda i: (place(i), 0, 0, 0))
     return pl.pallas_call(
         read_kernel,
-        grid=(width // step,),
+        grid=(steps,),
         in_specs=[
             wide,
             wide,
             wide,
-            pl.BlockSpec((1, step), lambda i: (0, i)),
-            pl.BlockSpec((count // 2, 2, PAIR, 2 * length), lambda i: (i, 0, 0, 0)),
-            per_head,
+            pl.BlockSpec((1, step), lambda i: (0, at(i))),
+            pl.BlockSpec((count // 2, 2, PAIR, 2 * length), lambda i: (at(i), 0, 0, 0)),
+            per_head(at),
         ],
-        out_specs=per_head,
+        out_specs=per_head(lambda i: i),
         out_shape=jax.ShapeDtypeStruct((heads, 2, length, PAIR), BF16),
         name="chunk_reads",
-        **budget(60, 8),
+        **budget(60, 4),
     )(q, v, scale, centre, right, inner)
 
 
@@ -401,12 +418,12 @@
     )(msg)
 
 
-def finish(starts, reads, gain, weight):
-    length = reads.shape[2]
+def finish(starts, early, late, gain, weight):
+    length = early.shape[2]
     width = gain.shape[0]
     return pl.pallas_call(
         finish_kernel,
-        in_specs=[pl.BlockSpec(memory_space=pltpu.VMEM)] * 3 + [pl.BlockSpec(memory_space=pltpu.HBM)],
+        in_specs=[pl.BlockSpec(memory_space=pltpu.VMEM)] * 4 + [pl.BlockSpec(memory_space=pltpu.HBM)],
         out_shape=jax.ShapeDtypeStruct((length, weight.shape[0] * weight.shape[2]), BF16),
         scratch_shapes=[
             pltpu.VMEM((length, width), BF16),
@@ -414,8 +431,8 @@
             pltpu.SemaphoreType.DMA((weight.shape[0],)),
         ],
         name="finish",
-        **budget(60, 12),
-    )(starts, reads, gain.reshape(1, width), weight)
+        **budget(52, 6),
+    )(starts, early, late, gain.reshape(1, width), weight)
 
 
 def per_device(
@@ -425,12 +442,14 @@
     msg, inner, right, scale, centre = local_chunk(
         key_rows[0], value_rows[0], decay_low[0], rate_low[0], decay_up, rate_up, decay_base
     )
+    reads = (query_rows[0], value_rows[0], scale, centre, right, inner)
     here = lax.all_to_all(msg, "sp", split_axis=0, concat_axis=0, tiled=True)
-    reads = chunk_reads(query_rows[0], value_rows[0], scale, centre, right, inner)
-    here, reads = lax.optimization_barrier((here, reads))
+    early = chunk_reads(0, 2, *reads)
+    here, early = lax.optimization_barrier((here, early))
     starts = scan_chunks(here)
     back = lax.all_to_all(starts, "sp", split_axis=0, concat_axis=0, tiled=True)
-    return finish(back, reads, norm_gain, columns)[None]
+    late = chunk_reads(1, 2, *reads)
+    return finish(back, early, late, norm_gain, columns)[None]
 
 
 def solution(mesh):

time: 87.4 us -> 87.6 us (level)
  blocking collectives: 15.6 us -> 0 us
  waiting for transfers between devices: 11.2 us -> 21 us
  starting transfers between devices: 13.7 us -> 19.2 us
    all_to_all x1 -> x0, blocking collectives: 15.6 us -> none  [per_device(): back = lax.all_to_all(starts, 'sp', split_axis=0, concat_axis=0, tiled=True)]
    all_to_all x0 -> x1, waiting for transfers between devices: none -> 6.14 us  [per_device(): back = lax.all_to_all(starts, 'sp', split_axis=0, concat_axis=0, tiled=True)]
    all_to_all x0 -> x1, starting transfers between devices: none -> 5.43 us  [per_device(): back = lax.all_to_all(starts, 'sp', split_axis=0, concat_axis=0, tiled=True)]
    all_to_all x1, waiting for transfers between devices: 7.85 us -> 12.3 us  [per_device(): here = lax.all_to_all(msg, 'sp', split_axis=0, concat_axis=0, tiled=True)]
    pallas_call x1 -> x2, Pallas kernels: 8.43 us -> 8.01 us  [chunk_reads(): pl.pallas_call(read_kernel, grid=(steps,), in_specs=[wide, wide, wide, pl...]
  transfers between devices with their start and end apart: 2 -> 3, of which waited for: 2 -> 3; matrix products, arithmetic and copies ran while one was open for 0% -> 0% of each run, Pallas kernels for 30% -> 31%
where the time goes in v4:
time: 87.6 us; the launch traced here: 86.8 us
  Pallas kernels  33.2 us (38%)
  waiting for transfers between devices  21 us (24%)
  starting transfers between devices  19.2 us (22%)
  between operations  13.4 us (15%)
    pallas_call x1, Pallas kernels, local_chunk(): pl.pallas_call(local_kernel, grid=(width // step,), in_specs=[wide, wide,...  14.3 us
    all_to_all x1, starting transfers between devices, per_device(): here = lax.all_to_all(msg, 'sp', split_axis=0, concat_axis=0, tiled=True)  13.7 us
    all_to_all x1, waiting for transfers between devices, per_device(): here = lax.all_to_all(msg, 'sp', split_axis=0, concat_axis=0, tiled=True)  12.3 us
    pallas_call x2, Pallas kernels, chunk_reads(): pl.pallas_call(read_kernel, grid=(steps,), in_specs=[wide, wide, wide, pl...  8.01 us
    pallas_call x1, Pallas kernels, finish(): pl.pallas_call(finish_kernel, in_specs=[pl.BlockSpec(memory_space=pltpu.V...  6.38 us
    all_to_all x1, waiting for transfers between devices, per_device(): back = lax.all_to_all(starts, 'sp', split_axis=0, concat_axis=0, tiled=True)  6.14 us
    all_to_all x1, starting transfers between devices, per_device(): back = lax.all_to_all(starts, 'sp', split_axis=0, concat_axis=0, tiled=True)  5.43 us
    pallas_call x1, Pallas kernels, scan_chunks(): pl.pallas_call(scan_kernel, out_shape=jax.ShapeDtypeStruct((chunks, HEAD...  4.47 us
  transfers between devices with their start and end apart: 3, of which 3 were waited for; matrix products, arithmetic and copies ran while one was open for 0% of the time, Pallas kernels for 31%

profile of v4, /device:TPU:1, one launch (start us, length us, event | category | flops | bytes accessed | tf_op | source)
XLA Modules:
  0.0 86.8 jit_solution(12690112547322682286)
XLA Ops:
  6.5 0.0 all-gather.3.cloned.1.call-start
  6.5 0.7 all-gather.3.cloned.1.call-update
  7.3 14.3 %local_chunk.1 = (bf16[32,64,128]{2,1,0:T(8,128)(2,1)}, bf16[32,2,128,128]{3,2,1,0:T(8,128)(2,1)}, bf16[16,2,128,256]{3,2,1,0:T(8,128)(2,1)}, f32[128,2048]{1,0:T(8,128)}, f32[1,2048]{1,0:T(1,128)}) custom-call(bf16[128,2048]{1,0:T(8,128)(2,1)} %bitcast.11, bf16[128,2048]{1,0:T(8,128)(2,1)} %bitcast.12, bf16[128,128]{1,0:T(8,128)(2,1)} %bitcast.17, ...), custom_call_target="tpu_custom_call" | custom-call | flops 12499999744 | bytes 1048576 | tf_op jit(solution)/shard_map/local_chunk/pallas_call | solution.py:360
  21.6 13.7 %all-to-all-start = ((bf16[32,64,128]{2,1,0:T(8,128)(2,1)}), bf16[32,64,128]{2,1,0:T(8,128)(2,1)S(1)}, u32[]{:S(2)}, u32[]{:S(2)}) async-start(bf16[32,64,128]{2,1,0:T(8,128)(2,1)} %get-tuple-element.12), calls=%async_computation | async-start | bytes 1048576 | tf_op jit(solution)/shard_map/all_to_all | solution.py:446
  35.3 3.9 %chunk_reads.2.early_ref = bf16[16,2,128,128]{3,2,1,0:T(8,128)(2,1)} custom-call(bf16[128,2048]{1,0:T(8,128)(2,1)} %bitcast.15, bf16[128,2048]{1,0:T(8,128)(2,1)} %bitcast.13, f32[128,2048]{1,0:T(8,128)} %get-tuple-element.13.scale_ref, f32[1,2048]{1,0:T(1,128)} %get-tuple-element.14.centre_ref, bf16[16,2,128,256]{3,2,1,0:T(8,128)(2,1)} %get-tuple-element.15.right_ref, ...), custom_call_target="tpu_custom_call" | custom-call | flops 2000000000 | bytes 1048576 | tf_op jit(solution)/shard_map/chunk_reads/pallas_call | solution.py:393
  39.3 12.3 %all-to-all-done.msg_ref = bf16[32,64,128]{2,1,0:T(8,128)(2,1)S(1)} async-done(((bf16[32,64,128]{2,1,0:T(8,128)(2,1)}), bf16[32,64,128]{2,1,0:T(8,128)(2,1)S(1)}, u32[]{:S(2)}, u32[]{:S(2)}) %all-to-all-start) | async-done | bytes 524320 | tf_op jit(solution)/shard_map/all_to_all | solution.py:446
  51.6 4.5 %scan_chunks.1 = bf16[32,32,128]{2,1,0:T(8,128)(2,1)} custom-call(bf16[32,64,128]{2,1,0:T(8,128)(2,1)S(1)} %all-to-all-done.msg_ref), custom_call_target="tpu_custom_call" | custom-call | flops 3000000000 | bytes 1048576 | tf_op jit(solution)/shard_map/scan_chunks/pallas_call | solution.py:413
  56.1 5.4 %all-to-all-start.1 = ((bf16[32,32,128]{2,1,0:T(8,128)(2,1)}), bf16[32,32,128]{2,1,0:T(8,128)(2,1)S(1)}, u32[]{:S(2)}, u32[]{:S(2)}) async-start(bf16[32,32,128]{2,1,0:T(8,128)(2,1)} %scan_chunks.1), calls=%async_computation.1 | async-start | bytes 524288 | tf_op jit(solution)/shard_map/all_to_all | solution.py:450
  61.5 0.0 copy-start
  61.5 0.0 copy-start.1
  61.5 4.1 %chunk_reads.3.late_ref = bf16[16,2,128,128]{3,2,1,0:T(8,128)(2,1)} custom-call(bf16[128,2048]{1,0:T(8,128)(2,1)} %bitcast.16, bf16[128,2048]{1,0:T(8,128)(2,1)} %bitcast.14, f32[128,2048]{1,0:T(8,128)} %get-tuple-element.13.scale_ref, f32[1,2048]{1,0:T(1,128)} %get-tuple-element.14.centre_ref, bf16[16,2,128,256]{3,2,1,0:T(8,128)(2,1)} %get-tuple-element.15.right_ref, ...), custom_call_target="tpu_custom_call" | custom-call | flops 2000000000 | bytes 1048576 | tf_op jit(solution)/shard_map/chunk_reads/pallas_call | solution.py:393
  65.6 6.1 %all-to-all-done.1.start_ref = bf16[32,32,128]{2,1,0:T(8,128)(2,1)S(1)} async-done(((bf16[32,32,128]{2,1,0:T(8,128)(2,1)}), bf16[32,32,128]{2,1,0:T(8,128)(2,1)S(1)}, u32[]{:S(2)}, u32[]{:S(2)}) %all-to-all-start.1) | async-done | bytes 262176 | tf_op jit(solution)/shard_map/all_to_all | solution.py:450
  71.7 1.8 %all-gather.3.cloned.1.call-done = bf16[32768,128]{1,0:T(8,128)(2,1)} async-done(((bf16[2048,128]{1,0:T(8,128)(2,1)}), bf16[32768,128]{1,0:T(8,128)(2,1)}) %all-gather.3.cloned.1.call-update) | async-done | bytes 8388624 | tf_op jit(solution)/shard_map/all_gather | solution.py:441
  73.5 0.0 copy-done
  73.5 0.0 copy-done.1
  73.5 6.4 %finish.1 = bf16[128,2048]{1,0:T(8,128)(2,1)} custom-call(bf16[32,32,128]{2,1,0:T(8,128)(2,1)S(1)} %all-to-all-done.1.start_ref, bf16[16,2,128,128]{3,2,1,0:T(8,128)(2,1)S(1)} %copy-done, bf16[16,2,128,128]{3,2,1,0:T(8,128)(2,1)} %chunk_reads.3.late_ref, f32[1,2048]{1,0:T(1,128)S(1)} %bitcast.9, bf16[16,2048,128]{2,1,0:T(8,128)(2,1)} %bitcast.10), custom_call_target="tpu_custom_call" | custom-call | flops 3000000000 | bytes 1048576 | tf_op jit(solution)/shard_map/finish/pallas_call | solution.py:424
Async XLA Ops:
  6.5 67.0 %all-gather.3.cloned.1.call-start = ((), (), s32[]{:S(2)}) async-start(), calls=%async_computation.2 | async-start | bytes 8912896 | tf_op jit(solution)/shard_map/all_gather | solution.py:441
  21.6 30.0 %all-to-all-start = ((bf16[32,64,128]{2,1,0:T(8,128)(2,1)}), bf16[32,64,128]{2,1,0:T(8,128)(2,1)S(1)}, u32[]{:S(2)}, u32[]{:S(2)}) async-start(bf16[32,64,128]{2,1,0:T(8,128)(2,1)} %get-tuple-element.12), calls=%async_computation | async-start | bytes 1048576 | tf_op jit(solution)/shard_map/all_to_all | solution.py:446
  56.1 15.7 %all-to-all-start.1 = ((bf16[32,32,128]{2,1,0:T(8,128)(2,1)}), bf16[32,32,128]{2,1,0:T(8,128)(2,1)S(1)}, u32[]{:S(2)}, u32[]{:S(2)}) async-start(bf16[32,32,128]{2,1,0:T(8,128)(2,1)} %scan_chunks.1), calls=%async_computation.1 | async-start | bytes 524288 | tf_op jit(solution)/shard_map/all_to_all | solution.py:450
  61.5 12.0 %copy-start = (bf16[16,2,128,128]{3,2,1,0:T(8,128)(2,1)S(1)}, bf16[16,2,128,128]{3,2,1,0:T(8,128)(2,1)}, u32[]{:S(2)}) copy-start(bf16[16,2,128,128]{3,2,1,0:T(8,128)(2,1)} %chunk_reads.2.early_ref) | copy-start | bytes 3145732
  61.5 12.0 %copy-start.1 = (f32[2048]{0:T(1024)S(1)}, f32[2048]{0:T(1024)}, u32[]{:S(2)}) copy-start(f32[2048]{0:T(1024)} %param.18) | copy-start | bytes 24580
Sparse Core Ops, SparseCore 0:
  9.4 64.0 all-gather.2

commit v5 on v4

--- a/solution.py
+++ b/solution.py
@@ -13,6 +13,7 @@
 GROUP = 16
 TOGETHER = 8
 ABREAST = 8
+RUN = 8
 READS = 4
 BLOCKS = 4
 FLOPS_PER_US = 500_000_000
@@ -276,20 +277,47 @@
 
 
 def scan_kernel(msg_ref, start_ref):
-    first = iota((HEAD, PAIR), 1) < HEAD
-    eye = (iota((HEAD, PAIR), 0) + HEAD == iota((HEAD, PAIR), 1)).astype(F32).astype(BF16)
-    nothing = jnp.zeros((HEAD, PAIR), BF16)
-    state = jnp.zeros((HEAD, PAIR), F32)
     chunks = msg_ref.shape[0]
+    runs = chunks // RUN
     half = HEAD // 2
-    for i in range(chunks):
+    first = iota((PAIR, PAIR), 1) < HEAD
+    eye = (iota((PAIR, PAIR), 0) + HEAD == iota((PAIR, PAIR), 1)).astype(F32).astype(BF16)
+    nothing = jnp.zeros((PAIR, PAIR), BF16)
+    begin = (iota((PAIR, PAIR), 0) == HEAD + (iota((PAIR, PAIR), 1) % HEAD)).astype(F32)
+
+    def put(i, state):
         start_ref[i] = jnp.where(first[:half], state[:half], state[half:]).astype(BF16)
-        if i + 1 < chunks:
-            high, low = split(state)
-            left = lanes(jnp.where(first, high, eye), jnp.where(first, low, nothing))
-            here = msg_ref[i]
+
+    held = [[begin if r else begin[:HEAD]] for r in range(runs)]
+    parts = [[split(h[0])] for h in held]
+    for j in range(RUN):
+        for r in range(runs):
+            if j + 1 == RUN and r + 1 == runs:
+                continue
+            high, low = parts[r][j]
+            tall = high.shape[0]
+            left = lanes(jnp.where(first[:tall], high, eye[:tall]), jnp.where(first[:tall], low, nothing[:tall]))
+            here = msg_ref[r * RUN + j]
             here = rows(here, here)
-            state = state + dot_nt(left, lanes(here, here))
+            held[r].append(held[r][j] + dot_nt(left, lanes(here, here)))
+            parts[r].append(split(held[r][j + 1]))
+    for j in range(RUN):
+        put(j, held[0][j])
+    state = held[0][RUN]
+    for r in range(1, runs):
+        put(r * RUN, state)
+        high, low = split(state)
+        blank = nothing[:HEAD]
+        left = lanes(jnp.where(first[:HEAD], high, low), jnp.where(first[:HEAD], high, blank))
+        for j in range(RUN, 0, -1):
+            if j == RUN and r + 1 == runs:
+                continue
+            high, low = (x[HEAD:] for x in parts[r][j])
+            moved = held[r][j][:HEAD] + dot(left, rows(high, high, low, blank))
+            if j == RUN:
+                state = moved
+            else:
+                put(r * RUN + j, moved)
 
 
 def finish_kernel(start_ref, early_ref, late_ref, gain_ref, w_ref, out_ref, mix_ref, here_ref, done_ref):

time: 87.6 us -> 87.1 us (level)
  Pallas kernels: 33.2 us -> 31 us
  waiting for transfers between devices: 21 us -> 23.2 us
    all_gather x1, waiting for transfers between devices: 1.8 us -> 3.99 us  [per_device(): columns = lax.all_gather(out_weight, DP)]
    pallas_call x1, Pallas kernels: 4.47 us -> 2.29 us  [scan_chunks(): pl.pallas_call(scan_kernel, out_shape=jax.ShapeDtypeStruct((chunks, HEAD...]
  transfers between devices with their start and end apart: 3 -> 3, of which waited for: 3 -> 3; matrix products, arithmetic and copies ran while one was open for 0% -> 0% of each run, Pallas kernels for 31% -> 28%
where the time goes in v5:
time: 87.1 us; the launch traced here: 86.8 us
  Pallas kernels  31 us (36%)
  waiting for transfers between devices  23.2 us (27%)
  starting transfers between devices  19.2 us (22%)
  between operations  13.4 us (15%)
    pallas_call x1, Pallas kernels, local_chunk(): pl.pallas_call(local_kernel, grid=(width // step,), in_specs=[wide, wide,...  14.3 us
    all_to_all x1, starting transfers between devices, per_device(): here = lax.all_to_all(msg, 'sp', split_axis=0, concat_axis=0, tiled=True)  13.7 us
    all_to_all x1, waiting for transfers between devices, per_device(): here = lax.all_to_all(msg, 'sp', split_axis=0, concat_axis=0, tiled=True)  12.3 us
    pallas_call x2, Pallas kernels, chunk_reads(): pl.pallas_call(read_kernel, grid=(steps,), in_specs=[wide, wide, wide, pl...  7.96 us
    pallas_call x1, Pallas kernels, finish(): pl.pallas_call(finish_kernel, in_specs=[pl.BlockSpec(memory_space=pltpu.V...  6.38 us
    all_to_all x1, waiting for transfers between devices, per_device(): back = lax.all_to_all(starts, 'sp', split_axis=0, concat_axis=0, tiled=True)  6.18 us
    all_to_all x1, starting transfers between devices, per_device(): back = lax.all_to_all(starts, 'sp', split_axis=0, concat_axis=0, tiled=True)  5.43 us
    all_gather x1, waiting for transfers between devices, per_device(): columns = lax.all_gather(out_weight, DP)  3.99 us
  transfers between devices with their start and end apart: 3, of which 3 were waited for; matrix products, arithmetic and copies ran while one was open for 0% of the time, Pallas kernels for 28%

profile of v5, /device:TPU:1, one launch (start us, length us, event | category | flops | bytes accessed | tf_op | source)
XLA Modules:
  0.0 86.8 jit_solution(11598925600359768239)
XLA Ops:
  6.5 0.0 all-gather.3.cloned.1.call-start
  6.5 0.7 all-gather.3.cloned.1.call-update
  7.3 14.3 %local_chunk.1 = (bf16[32,64,128]{2,1,0:T(8,128)(2,1)}, bf16[32,2,128,128]{3,2,1,0:T(8,128)(2,1)}, bf16[16,2,128,256]{3,2,1,0:T(8,128)(2,1)}, f32[128,2048]{1,0:T(8,128)}, f32[1,2048]{1,0:T(1,128)}) custom-call(bf16[128,2048]{1,0:T(8,128)(2,1)} %bitcast.11, bf16[128,2048]{1,0:T(8,128)(2,1)} %bitcast.12, bf16[128,128]{1,0:T(8,128)(2,1)} %bitcast.17, ...), custom_call_target="tpu_custom_call" | custom-call | flops 12499999744 | bytes 1048576 | tf_op jit(solution)/shard_map/local_chunk/pallas_call | solution.py:388
  21.6 13.7 %all-to-all-start = ((bf16[32,64,128]{2,1,0:T(8,128)(2,1)}), bf16[32,64,128]{2,1,0:T(8,128)(2,1)S(1)}, u32[]{:S(2)}, u32[]{:S(2)}) async-start(bf16[32,64,128]{2,1,0:T(8,128)(2,1)} %get-tuple-element.12), calls=%async_computation | async-start | bytes 1048576 | tf_op jit(solution)/shard_map/all_to_all | solution.py:474
  35.3 3.9 %chunk_reads.2.early_ref = bf16[16,2,128,128]{3,2,1,0:T(8,128)(2,1)} custom-call(bf16[128,2048]{1,0:T(8,128)(2,1)} %bitcast.15, bf16[128,2048]{1,0:T(8,128)(2,1)} %bitcast.13, f32[128,2048]{1,0:T(8,128)} %get-tuple-element.13.scale_ref, f32[1,2048]{1,0:T(1,128)} %get-tuple-element.14.centre_ref, bf16[16,2,128,256]{3,2,1,0:T(8,128)(2,1)} %get-tuple-element.15.right_ref, ...), custom_call_target="tpu_custom_call" | custom-call | flops 2000000000 | bytes 1048576 | tf_op jit(solution)/shard_map/chunk_reads/pallas_call | solution.py:421
  39.3 12.3 %all-to-all-done.msg_ref = bf16[32,64,128]{2,1,0:T(8,128)(2,1)S(1)} async-done(((bf16[32,64,128]{2,1,0:T(8,128)(2,1)}), bf16[32,64,128]{2,1,0:T(8,128)(2,1)S(1)}, u32[]{:S(2)}, u32[]{:S(2)}) %all-to-all-start) | async-done | bytes 524320 | tf_op jit(solution)/shard_map/all_to_all | solution.py:474
  51.6 2.3 %scan_chunks.1 = bf16[32,32,128]{2,1,0:T(8,128)(2,1)} custom-call(bf16[32,64,128]{2,1,0:T(8,128)(2,1)S(1)} %all-to-all-done.msg_ref), custom_call_target="tpu_custom_call" | custom-call | flops 3000000000 | bytes 1048576 | tf_op jit(solution)/shard_map/scan_chunks/pallas_call | solution.py:441
  53.9 5.4 %all-to-all-start.1 = ((bf16[32,32,128]{2,1,0:T(8,128)(2,1)}), bf16[32,32,128]{2,1,0:T(8,128)(2,1)S(1)}, u32[]{:S(2)}, u32[]{:S(2)}) async-start(bf16[32,32,128]{2,1,0:T(8,128)(2,1)} %scan_chunks.1), calls=%async_computation.1 | async-start | bytes 524288 | tf_op jit(solution)/shard_map/all_to_all | solution.py:478
  59.3 0.0 copy-start
  59.3 0.0 copy-start.1
  59.4 4.0 %chunk_reads.3.late_ref = bf16[16,2,128,128]{3,2,1,0:T(8,128)(2,1)} custom-call(bf16[128,2048]{1,0:T(8,128)(2,1)} %bitcast.16, bf16[128,2048]{1,0:T(8,128)(2,1)} %bitcast.14, f32[128,2048]{1,0:T(8,128)} %get-tuple-element.13.scale_ref, f32[1,2048]{1,0:T(1,128)} %get-tuple-element.14.centre_ref, bf16[16,2,128,256]{3,2,1,0:T(8,128)(2,1)} %get-tuple-element.15.right_ref, ...), custom_call_target="tpu_custom_call" | custom-call | flops 2000000000 | bytes 1048576 | tf_op jit(solution)/shard_map/chunk_reads/pallas_call | solution.py:421
  63.4 6.2 %all-to-all-done.1.start_ref = bf16[32,32,128]{2,1,0:T(8,128)(2,1)S(1)} async-done(((bf16[32,32,128]{2,1,0:T(8,128)(2,1)}), bf16[32,32,128]{2,1,0:T(8,128)(2,1)S(1)}, u32[]{:S(2)}, u32[]{:S(2)}) %all-to-all-start.1) | async-done | bytes 262176 | tf_op jit(solution)/shard_map/all_to_all | solution.py:478
  69.6 4.0 %all-gather.3.cloned.1.call-done = bf16[32768,128]{1,0:T(8,128)(2,1)} async-done(((bf16[2048,128]{1,0:T(8,128)(2,1)}), bf16[32768,128]{1,0:T(8,128)(2,1)}) %all-gather.3.cloned.1.call-update) | async-done | bytes 8388624 | tf_op jit(solution)/shard_map/all_gather | solution.py:469
  73.5 0.0 copy-done
  73.5 0.0 copy-done.1
  73.5 6.4 %finish.1 = bf16[128,2048]{1,0:T(8,128)(2,1)} custom-call(bf16[32,32,128]{2,1,0:T(8,128)(2,1)S(1)} %all-to-all-done.1.start_ref, bf16[16,2,128,128]{3,2,1,0:T(8,128)(2,1)S(1)} %copy-done, bf16[16,2,128,128]{3,2,1,0:T(8,128)(2,1)} %chunk_reads.3.late_ref, f32[1,2048]{1,0:T(1,128)S(1)} %bitcast.9, bf16[16,2048,128]{2,1,0:T(8,128)(2,1)} %bitcast.10), custom_call_target="tpu_custom_call" | custom-call | flops 3000000000 | bytes 1048576 | tf_op jit(solution)/shard_map/finish/pallas_call | solution.py:452
Async XLA Ops:
  6.5 67.0 %all-gather.3.cloned.1.call-start = ((), (), s32[]{:S(2)}) async-start(), calls=%async_computation.2 | async-start | bytes 8912896 | tf_op jit(solution)/shard_map/all_gather | solution.py:469
  21.6 30.0 %all-to-all-start = ((bf16[32,64,128]{2,1,0:T(8,128)(2,1)}), bf16[32,64,128]{2,1,0:T(8,128)(2,1)S(1)}, u32[]{:S(2)}, u32[]{:S(2)}) async-start(bf16[32,64,128]{2,1,0:T(8,128)(2,1)} %get-tuple-element.12), calls=%async_computation | async-start | bytes 1048576 | tf_op jit(solution)/shard_map/all_to_all | solution.py:474
  53.9 15.7 %all-to-all-start.1 = ((bf16[32,32,128]{2,1,0:T(8,128)(2,1)}), bf16[32,32,128]{2,1,0:T(8,128)(2,1)S(1)}, u32[]{:S(2)}, u32[]{:S(2)}) async-start(bf16[32,32,128]{2,1,0:T(8,128)(2,1)} %scan_chunks.1), calls=%async_computation.1 | async-start | bytes 524288 | tf_op jit(solution)/shard_map/all_to_all | solution.py:478
  59.3 14.2 %copy-start = (bf16[16,2,128,128]{3,2,1,0:T(8,128)(2,1)S(1)}, bf16[16,2,128,128]{3,2,1,0:T(8,128)(2,1)}, u32[]{:S(2)}) copy-start(bf16[16,2,128,128]{3,2,1,0:T(8,128)(2,1)} %chunk_reads.2.early_ref) | copy-start | bytes 3145732
  59.3 14.2 %copy-start.1 = (f32[2048]{0:T(1024)S(1)}, f32[2048]{0:T(1024)}, u32[]{:S(2)}) copy-start(f32[2048]{0:T(1024)} %param.18) | copy-start | bytes 24580
Sparse Core Ops, SparseCore 0:
  9.4 64.0 all-gather.2

commit v6 on v5

--- a/solution.py
+++ b/solution.py
@@ -320,7 +320,7 @@
                 put(r * RUN + j, moved)
 
 
-def finish_kernel(start_ref, early_ref, late_ref, gain_ref, w_ref, out_ref, mix_ref, here_ref, done_ref):
+def finish_kernel(start_ref, read_ref, gain_ref, w_ref, out_ref, mix_ref, here_ref, done_ref):
     copies = [pltpu.make_async_copy(w_ref.at[k], here_ref.at[k], done_ref.at[k]) for k in range(w_ref.shape[0])]
     for copy in copies:
         copy.start()
@@ -344,9 +344,7 @@
         ).T
         right = rows(states[:HEAD], eyes[0], states[HEAD:], eyes[1]).astype(BF16)
         yield
-        early = early_ref.shape[0] // 2
-        read_ref, q = (early_ref, p) if p < early else (late_ref, p - early)
-        left = rows(*(lanes(read_ref[2 * q, part], read_ref[2 * q + 1, part]) for part in range(2)))
+        left = rows(*(lanes(read_ref[2 * p, part], read_ref[2 * p + 1, part]) for part in range(2)))
         readout = dot(left, right)
         yield
         readout = readout[:length] + readout[length:]
@@ -409,13 +407,13 @@
     )(k, v, dl, rl, du, ru, base.reshape(1, width))
 
 
-def chunk_reads(part, parts, q, v, scale, centre, right, inner):
+def chunk_reads(q, v, scale, centre, right, inner):
     length, width = q.shape
-    heads = width // HEAD // parts
+    heads = width // HEAD
     count = GROUP // 2
     step = count * HEAD
     steps = heads // count
-    at = lambda i: part * steps + i
+    at = lambda i: i
     wide = pl.BlockSpec((length, step), lambda i: (0, at(i)))
     per_head = lambda place: pl.BlockSpec((count, 2, length, PAIR), lambda i: (place(i), 0, 0, 0))
     return pl.pallas_call(
@@ -432,7 +430,7 @@
         out_specs=per_head(lambda i: i),
         out_shape=jax.ShapeDtypeStruct((heads, 2, length, PAIR), BF16),
         name="chunk_reads",
-        **budget(60, 4),
+        **budget(60, 8),
     )(q, v, scale, centre, right, inner)
 
 
@@ -446,12 +444,12 @@
     )(msg)
 
 
-def finish(starts, early, late, gain, weight):
-    length = early.shape[2]
+def finish(starts, reads, gain, weight):
+    length = reads.shape[2]
     width = gain.shape[0]
     return pl.pallas_call(
         finish_kernel,
-        in_specs=[pl.BlockSpec(memory_space=pltpu.VMEM)] * 4 + [pl.BlockSpec(memory_space=pltpu.HBM)],
+        in_specs=[pl.BlockSpec(memory_space=pltpu.VMEM)] * 3 + [pl.BlockSpec(memory_space=pltpu.HBM)],
         out_shape=jax.ShapeDtypeStruct((length, weight.shape[0] * weight.shape[2]), BF16),
         scratch_shapes=[
             pltpu.VMEM((length, width), BF16),
@@ -459,8 +457,8 @@
             pltpu.SemaphoreType.DMA((weight.shape[0],)),
         ],
         name="finish",
-        **budget(52, 6),
-    )(starts, early, late, gain.reshape(1, width), weight)
+        **budget(60, 6),
+    )(starts, reads, gain.reshape(1, width), weight)
 
 
 def per_device(
@@ -472,12 +470,11 @@
     )
     reads = (query_rows[0], value_rows[0], scale, centre, right, inner)
     here = lax.all_to_all(msg, "sp", split_axis=0, concat_axis=0, tiled=True)
-    early = chunk_reads(0, 2, *reads)
-    here, early = lax.optimization_barrier((here, early))
+    read = chunk_reads(*reads)
+    here, read = lax.optimization_barrier((here, read))
     starts = scan_chunks(here)
     back = lax.all_to_all(starts, "sp", split_axis=0, concat_axis=0, tiled=True)
-    late = chunk_reads(1, 2, *reads)
-    return finish(back, early, late, norm_gain, columns)[None]
+    return finish(back, read, norm_gain, columns)[None]
 
 
 def solution(mesh):

time: 87.1 us -> 87.1 us (level)
  blocking collectives: 0 us -> 15.6 us
  waiting for transfers between devices: 23.2 us -> 15.4 us
  starting transfers between devices: 19.2 us -> 13.7 us
  Pallas kernels: 31 us -> 28.7 us
    all_to_all x0 -> x1, blocking collectives: none -> 15.6 us  [per_device(): back = lax.all_to_all(starts, 'sp', split_axis=0, concat_axis=0, tiled=True)]
    all_to_all x1 -> x0, waiting for transfers between devices: 6.18 us -> none  [per_device(): back = lax.all_to_all(starts, 'sp', split_axis=0, concat_axis=0, tiled=True)]
    all_to_all x1 -> x0, starting transfers between devices: 5.43 us -> none  [per_device(): back = lax.all_to_all(starts, 'sp', split_axis=0, concat_axis=0, tiled=True)]
    all_to_all x1, waiting for transfers between devices: 12.3 us -> 9.86 us  [per_device(): here = lax.all_to_all(msg, 'sp', split_axis=0, concat_axis=0, tiled=True)]
    pallas_call x2 -> x1, Pallas kernels: 7.96 us -> 6.43 us  [chunk_reads(): pl.pallas_call(read_kernel, grid=(steps,), in_specs=[wide, wide, wide, pl...]
  transfers between devices with their start and end apart: 3 -> 2, of which waited for: 3 -> 2; matrix products, arithmetic and copies ran while one was open for 0% -> 0% of each run, Pallas kernels for 28% -> 26%
where the time goes in v6:
time: 87.1 us; the launch traced here: 86.7 us
  Pallas kernels  28.7 us (33%)
  blocking collectives  15.6 us (18%)
  waiting for transfers between devices  15.4 us (18%)
  starting transfers between devices  13.7 us (16%)
  between operations  13.4 us (15%)
    all_to_all x1, blocking collectives, per_device(): back = lax.all_to_all(starts, 'sp', split_axis=0, concat_axis=0, tiled=True)  15.6 us
    pallas_call x1, Pallas kernels, local_chunk(): pl.pallas_call(local_kernel, grid=(width // step,), in_specs=[wide, wide,...  14.3 us
    all_to_all x1, starting transfers between devices, per_device(): here = lax.all_to_all(msg, 'sp', split_axis=0, concat_axis=0, tiled=True)  13.7 us
    all_to_all x1, waiting for transfers between devices, per_device(): here = lax.all_to_all(msg, 'sp', split_axis=0, concat_axis=0, tiled=True)  9.86 us
    pallas_call x1, Pallas kernels, chunk_reads(): pl.pallas_call(read_kernel, grid=(steps,), in_specs=[wide, wide, wide, pl...  6.43 us
    pallas_call x1, Pallas kernels, finish(): pl.pallas_call(finish_kernel, in_specs=[pl.BlockSpec(memory_space=pltpu.V...  6.34 us
    all_gather x1, waiting for transfers between devices, per_device(): columns = lax.all_gather(out_weight, DP)  4.79 us
  transfers between devices with their start and end apart: 2, of which 2 were waited for; matrix products, arithmetic and copies ran while one was open for 0% of the time, Pallas kernels for 26%

profile of v6, /device:TPU:1, one launch (start us, length us, event | category | flops | bytes accessed | tf_op | source)
XLA Modules:
  0.0 86.7 jit_solution(9597303444248963198)
XLA Ops:
  6.5 0.0 all-gather.3.cloned.1.call-start
  6.5 0.7 all-gather.3.cloned.1.call-update
  7.3 14.3 %local_chunk.1 = (bf16[32,64,128]{2,1,0:T(8,128)(2,1)}, bf16[32,2,128,128]{3,2,1,0:T(8,128)(2,1)}, bf16[16,2,128,256]{3,2,1,0:T(8,128)(2,1)}, f32[128,2048]{1,0:T(8,128)}, f32[1,2048]{1,0:T(1,128)}) custom-call(bf16[128,2048]{1,0:T(8,128)(2,1)} %bitcast.11, bf16[128,2048]{1,0:T(8,128)(2,1)} %bitcast.12, bf16[128,128]{1,0:T(8,128)(2,1)} %bitcast.15, ...), custom_call_target="tpu_custom_call" | custom-call | flops 12499999744 | bytes 1048576 | tf_op jit(solution)/shard_map/local_chunk/pallas_call | solution.py:386
  21.6 13.7 %all-to-all-start = ((bf16[32,64,128]{2,1,0:T(8,128)(2,1)}), bf16[32,64,128]{2,1,0:T(8,128)(2,1)S(1)}, u32[]{:S(2)}, u32[]{:S(2)}) async-start(bf16[32,64,128]{2,1,0:T(8,128)(2,1)} %get-tuple-element.12), calls=%async_computation | async-start | bytes 1048576 | tf_op jit(solution)/shard_map/all_to_all | solution.py:472
  35.3 6.4 %chunk_reads.1.read_ref = bf16[32,2,128,128]{3,2,1,0:T(8,128)(2,1)} custom-call(bf16[128,2048]{1,0:T(8,128)(2,1)} %bitcast.14, bf16[128,2048]{1,0:T(8,128)(2,1)} %bitcast.13, f32[128,2048]{1,0:T(8,128)} %get-tuple-element.13.scale_ref, f32[1,2048]{1,0:T(1,128)} %get-tuple-element.14.centre_ref, bf16[16,2,128,256]{3,2,1,0:T(8,128)(2,1)} %get-tuple-element.15.right_ref, ...), custom_call_target="tpu_custom_call" | custom-call | flops 4000000000 | bytes 1048576 | tf_op jit(solution)/shard_map/chunk_reads/pallas_call | solution.py:419
  41.8 9.9 %all-to-all-done.msg_ref = bf16[32,64,128]{2,1,0:T(8,128)(2,1)S(1)} async-done(((bf16[32,64,128]{2,1,0:T(8,128)(2,1)}), bf16[32,64,128]{2,1,0:T(8,128)(2,1)S(1)}, u32[]{:S(2)}, u32[]{:S(2)}) %all-to-all-start) | async-done | bytes 524320 | tf_op jit(solution)/shard_map/all_to_all | solution.py:472
  51.6 1.6 %scan_chunks.1 = bf16[32,32,128]{2,1,0:T(8,128)(2,1)S(1)} custom-call(bf16[32,64,128]{2,1,0:T(8,128)(2,1)S(1)} %all-to-all-done.msg_ref), custom_call_target="tpu_custom_call" | custom-call | flops 3000000000 | bytes 1048576 | tf_op jit(solution)/shard_map/scan_chunks/pallas_call | solution.py:439
  53.2 15.6 %all_to_all.10.start_ref = bf16[32,32,128]{2,1,0:T(8,128)(2,1)} all-to-all(bf16[32,32,128]{2,1,0:T(8,128)(2,1)S(1)} %scan_chunks.1), channel_id=1, replica_groups=mesh['sp'=32,'dp_0'=8,'dp_1'=2] {'sp'}, dimensions={0} | all-to-all | bytes 524288 | tf_op jit(solution)/shard_map/all_to_all | solution.py:476
  68.8 4.8 %all-gather.3.cloned.1.call-done = bf16[32768,128]{1,0:T(8,128)(2,1)} async-done(((bf16[2048,128]{1,0:T(8,128)(2,1)}), bf16[32768,128]{1,0:T(8,128)(2,1)}) %all-gather.3.cloned.1.call-update) | async-done | bytes 8388624 | tf_op jit(solution)/shard_map/all_gather | solution.py:467
  73.5 6.3 %finish.1 = bf16[128,2048]{1,0:T(8,128)(2,1)} custom-call(bf16[32,32,128]{2,1,0:T(8,128)(2,1)} %all_to_all.10.start_ref, bf16[32,2,128,128]{3,2,1,0:T(8,128)(2,1)} %chunk_reads.1.read_ref, f32[1,2048]{1,0:T(1,128)} %bitcast.10, bf16[16,2048,128]{2,1,0:T(8,128)(2,1)} %bitcast.9), custom_call_target="tpu_custom_call" | custom-call | flops 3000000000 | bytes 1048576 | tf_op jit(solution)/shard_map/finish/pallas_call | solution.py:450
Async XLA Ops:
  6.5 67.0 %all-gather.3.cloned.1.call-start = ((), (), s32[]{:S(2)}) async-start(), calls=%async_computation.2 | async-start | bytes 8912896 | tf_op jit(solution)/shard_map/all_gather | solution.py:467
  21.6 30.0 %all-to-all-start = ((bf16[32,64,128]{2,1,0:T(8,128)(2,1)}), bf16[32,64,128]{2,1,0:T(8,128)(2,1)S(1)}, u32[]{:S(2)}, u32[]{:S(2)}) async-start(bf16[32,64,128]{2,1,0:T(8,128)(2,1)} %get-tuple-element.12), calls=%async_computation | async-start | bytes 1048576 | tf_op jit(solution)/shard_map/all_to_all | solution.py:472
Sparse Core Ops, SparseCore 0:
  9.4 64.0 all-gather.2

commit v7 on v6

--- a/solution.py
+++ b/solution.py
@@ -457,7 +457,7 @@
             pltpu.SemaphoreType.DMA((weight.shape[0],)),
         ],
         name="finish",
-        **budget(60, 6),
+        **budget(52, 6),
     )(starts, reads, gain.reshape(1, width), weight)
 
 

time: 87.1 us -> 87.3 us (level)
  no operation moved by 1% of the time
where the time goes in v7:
time: 87.3 us; the launch traced here: 86.9 us
  Pallas kernels  28.9 us (33%)
  waiting for transfers between devices  15.5 us (18%)
  blocking collectives  15.5 us (18%)
  starting transfers between devices  13.7 us (16%)
  between operations  13.4 us (15%)
    all_to_all x1, blocking collectives, per_device(): back = lax.all_to_all(starts, 'sp', split_axis=0, concat_axis=0, tiled=True)  15.5 us
    pallas_call x1, Pallas kernels, local_chunk(): pl.pallas_call(local_kernel, grid=(width // step,), in_specs=[wide, wide,...  14.3 us
    all_to_all x1, starting transfers between devices, per_device(): here = lax.all_to_all(msg, 'sp', split_axis=0, concat_axis=0, tiled=True)  13.7 us
    all_to_all x1, waiting for transfers between devices, per_device(): here = lax.all_to_all(msg, 'sp', split_axis=0, concat_axis=0, tiled=True)  9.85 us
    pallas_call x1, Pallas kernels, finish(): pl.pallas_call(finish_kernel, in_specs=[pl.BlockSpec(memory_space=pltpu.V...  6.53 us
    pallas_call x1, Pallas kernels, chunk_reads(): pl.pallas_call(read_kernel, grid=(steps,), in_specs=[wide, wide, wide, pl...  6.43 us
    all_gather x1, waiting for transfers between devices, per_device(): columns = lax.all_gather(out_weight, DP)  4.89 us
  transfers between devices with their start and end apart: 2, of which 2 were waited for; matrix products, arithmetic and copies ran while one was open for 0% of the time, Pallas kernels for 26%

profile of v7, /device:TPU:1, one launch (start us, length us, event | category | flops | bytes accessed | tf_op | source)
XLA Modules:
  0.0 86.9 jit_solution(5726179472356913929)
XLA Ops:
  6.5 0.0 all-gather.3.cloned.1.call-start
  6.5 0.7 all-gather.3.cloned.1.call-update
  7.3 14.3 %local_chunk.1 = (bf16[32,64,128]{2,1,0:T(8,128)(2,1)}, bf16[32,2,128,128]{3,2,1,0:T(8,128)(2,1)}, bf16[16,2,128,256]{3,2,1,0:T(8,128)(2,1)}, f32[128,2048]{1,0:T(8,128)}, f32[1,2048]{1,0:T(1,128)}) custom-call(bf16[128,2048]{1,0:T(8,128)(2,1)} %bitcast.11, bf16[128,2048]{1,0:T(8,128)(2,1)} %bitcast.12, bf16[128,128]{1,0:T(8,128)(2,1)} %bitcast.15, ...), custom_call_target="tpu_custom_call" | custom-call | flops 12499999744 | bytes 1048576 | tf_op jit(solution)/shard_map/local_chunk/pallas_call | solution.py:386
  21.6 13.7 %all-to-all-start = ((bf16[32,64,128]{2,1,0:T(8,128)(2,1)}), bf16[32,64,128]{2,1,0:T(8,128)(2,1)S(1)}, u32[]{:S(2)}, u32[]{:S(2)}) async-start(bf16[32,64,128]{2,1,0:T(8,128)(2,1)} %get-tuple-element.12), calls=%async_computation | async-start | bytes 1048576 | tf_op jit(solution)/shard_map/all_to_all | solution.py:472
  35.3 6.4 %chunk_reads.1.read_ref = bf16[32,2,128,128]{3,2,1,0:T(8,128)(2,1)} custom-call(bf16[128,2048]{1,0:T(8,128)(2,1)} %bitcast.14, bf16[128,2048]{1,0:T(8,128)(2,1)} %bitcast.13, f32[128,2048]{1,0:T(8,128)} %get-tuple-element.13.scale_ref, f32[1,2048]{1,0:T(1,128)} %get-tuple-element.14.centre_ref, bf16[16,2,128,256]{3,2,1,0:T(8,128)(2,1)} %get-tuple-element.15.right_ref, ...), custom_call_target="tpu_custom_call" | custom-call | flops 4000000000 | bytes 1048576 | tf_op jit(solution)/shard_map/chunk_reads/pallas_call | solution.py:419
  41.8 0.0 copy-start
  41.8 9.9 %all-to-all-done.msg_ref = bf16[32,64,128]{2,1,0:T(8,128)(2,1)S(1)} async-done(((bf16[32,64,128]{2,1,0:T(8,128)(2,1)}), bf16[32,64,128]{2,1,0:T(8,128)(2,1)S(1)}, u32[]{:S(2)}, u32[]{:S(2)}) %all-to-all-start) | async-done | bytes 524320 | tf_op jit(solution)/shard_map/all_to_all | solution.py:472
  51.6 1.6 %scan_chunks.1 = bf16[32,32,128]{2,1,0:T(8,128)(2,1)S(1)} custom-call(bf16[32,64,128]{2,1,0:T(8,128)(2,1)S(1)} %all-to-all-done.msg_ref), custom_call_target="tpu_custom_call" | custom-call | flops 3000000000 | bytes 1048576 | tf_op jit(solution)/shard_map/scan_chunks/pallas_call | solution.py:439
  53.2 15.5 %all_to_all.10.start_ref = bf16[32,32,128]{2,1,0:T(8,128)(2,1)S(1)} all-to-all(bf16[32,32,128]{2,1,0:T(8,128)(2,1)S(1)} %scan_chunks.1), channel_id=1, replica_groups=mesh['sp'=32,'dp_0'=8,'dp_1'=2] {'sp'}, dimensions={0} | all-to-all | bytes 524288 | tf_op jit(solution)/shard_map/all_to_all | solution.py:476
  68.6 4.9 %all-gather.3.cloned.1.call-done = bf16[32768,128]{1,0:T(8,128)(2,1)} async-done(((bf16[2048,128]{1,0:T(8,128)(2,1)}), bf16[32768,128]{1,0:T(8,128)(2,1)}) %all-gather.3.cloned.1.call-update) | async-done | bytes 8388624 | tf_op jit(solution)/shard_map/all_gather | solution.py:467
  73.5 0.0 copy-done
  73.5 6.5 %finish.1 = bf16[128,2048]{1,0:T(8,128)(2,1)} custom-call(bf16[32,32,128]{2,1,0:T(8,128)(2,1)S(1)} %all_to_all.10.start_ref, bf16[32,2,128,128]{3,2,1,0:T(8,128)(2,1)} %chunk_reads.1.read_ref, f32[1,2048]{1,0:T(1,128)S(1)} %bitcast.9, bf16[16,2048,128]{2,1,0:T(8,128)(2,1)} %bitcast.10), custom_call_target="tpu_custom_call" | custom-call | flops 3000000000 | bytes 1048576 | tf_op jit(solution)/shard_map/finish/pallas_call | solution.py:450
Async XLA Ops:
  6.5 67.0 %all-gather.3.cloned.1.call-start = ((), (), s32[]{:S(2)}) async-start(), calls=%async_computation.2 | async-start | bytes 8912896 | tf_op jit(solution)/shard_map/all_gather | solution.py:467
  21.6 30.0 %all-to-all-start = ((bf16[32,64,128]{2,1,0:T(8,128)(2,1)}), bf16[32,64,128]{2,1,0:T(8,128)(2,1)S(1)}, u32[]{:S(2)}, u32[]{:S(2)}) async-start(bf16[32,64,128]{2,1,0:T(8,128)(2,1)} %get-tuple-element.12), calls=%async_computation | async-start | bytes 1048576 | tf_op jit(solution)/shard_map/all_to_all | solution.py:472
  41.8 31.8 %copy-start = (f32[2048]{0:T(1024)S(1)}, f32[2048]{0:T(1024)}, u32[]{:S(2)}) copy-start(f32[2048]{0:T(1024)} %param.18) | copy-start | bytes 24580
Sparse Core Ops, SparseCore 0:
  9.4 64.0 all-gather.2
